TPU v7x, 32 devices: a whole 2x2x4 slice. The times are simulated.
32 devices in a mesh: fs: 16 (over z, y, x), tp: 2 (over core).
Axes of the slice: x: 2, y: 2, z: 4, core: 2. Of those that a mesh axis runs over, the one named last changes fastest.
Arguments:
- fwd_tokens: bfloat16 [2048, 2048], P('fs'), may hold values from -6 to 6
- back_tokens: bfloat16 [2048, 2048], P('fs'), may hold values from -6 to 6
- out_grad: bfloat16 [2048, 2048], P('fs'), may hold values from -6 to 6
- norm_gain: float32 [2048], replicated, may hold values from 0.1 to 1.9
- gate_weight: bfloat16 [2048, 2816], P('fs', 'tp'), may hold values from -0.125 to 0.125
- up_weight: bfloat16 [2048, 2816], P('fs', 'tp'), may hold values from -0.125 to 0.125
- down_weight: bfloat16 [2048, 2816], P('fs', 'tp'), may hold values from -0.109375 to 0.109375
- gate_grad_sum: float32 [2048, 2816], P('fs', 'tp'), may hold values from -96 to 96
Outputs:
- fwd_out: bfloat16 [2048, 2048], P('fs')
- back_grad: bfloat16 [2048, 2048], P('fs')
- gate_grad_out: float32 [2048, 2816], P('fs', 'tp')
All inputs are finite; a program needn't handle non-finite values.
Results may differ from a plain program's by a relative error of at most 0.014.
Values may be sent and summed in bfloat16 or wider, within the bound.
A program may use at most 64 MiB of HBM per device.

v0:
```python
import functools

import jax
import jax.numpy as jnp
from jax import lax
from jax.experimental import pallas as pl
from jax.experimental.pallas import tpu as pltpu
from jax.sharding import PartitionSpec as P

norm_eps = 0.25


def normalize(tokens, norm_gain):
    values = tokens.astype(jnp.float32)
    factor = lax.rsqrt(jnp.mean(values * values, axis=-1, keepdims=True) + norm_eps)
    return (values, factor, (values * factor * norm_gain).astype(jnp.bfloat16))


def shards(
    fwd_tokens, back_tokens, out_grad, norm_gain, gate_weight, up_weight, down_weight, gate_grad_sum
):
    fwd_normed = normalize(fwd_tokens, norm_gain)[2]
    columns = fwd_normed
    gate_pre = jnp.dot(
        columns,
        lax.all_gather(gate_weight, "fs", axis=0, tiled=True),
        preferred_element_type=jnp.float32,
    )
    up_pre = jnp.dot(
        columns,
        lax.all_gather(up_weight, "fs", axis=0, tiled=True),
        preferred_element_type=jnp.float32,
    )
    hidden = (gate_pre * jax.nn.sigmoid(gate_pre) * up_pre).astype(jnp.bfloat16)
    partial_value = jnp.dot(
        hidden,
        lax.all_gather(down_weight, "fs", axis=0, tiled=True).T,
        preferred_element_type=jnp.float32,
    )
    summed = lax.psum(partial_value.astype(jnp.bfloat16), "tp").astype(jnp.float32)
    fwd_out = (0.5 * summed).astype(jnp.bfloat16)
    gate_whole = lax.all_gather(gate_weight, "fs", axis=0, tiled=True)
    up_whole = lax.all_gather(up_weight, "fs", axis=0, tiled=True)
    down_whole = lax.all_gather(down_weight, "fs", axis=0, tiled=True)
    values, factor, back_normed = normalize(back_tokens, norm_gain)
    gate_pre = jnp.dot(back_normed, gate_whole, preferred_element_type=jnp.float32)
    up_pre = jnp.dot(back_normed, up_whole, preferred_element_type=jnp.float32)
    sigmoid_gate = jax.nn.sigmoid(gate_pre)
    back_hidden = 0.5 * jnp.dot(out_grad, down_whole, preferred_element_type=jnp.float32)
    gate_diff = (
        back_hidden * up_pre * sigmoid_gate * (1.0 + gate_pre * (1.0 - sigmoid_gate))
    ).astype(jnp.bfloat16)
    up_diff = (back_hidden * gate_pre * sigmoid_gate).astype(jnp.bfloat16)
    columns = back_normed
    gate_grad_out = gate_grad_sum + lax.psum_scatter(
        jnp.dot(columns.T, gate_diff, preferred_element_type=jnp.float32),
        "fs",
        scatter_dimension=0,
        tiled=True,
    )
    partial_diff = jnp.dot(gate_diff, gate_whole.T, preferred_element_type=jnp.float32)
    partial_diff = partial_diff + jnp.dot(up_diff, up_whole.T, preferred_element_type=jnp.float32)
    normed_diff = lax.psum(partial_diff.astype(jnp.bfloat16), "tp").astype(jnp.float32)
    scaled = normed_diff * norm_gain
    cubed = factor * factor * factor
    back_grad = (
        factor * scaled - values * cubed * jnp.mean(scaled * values, axis=-1, keepdims=True)
    ).astype(jnp.bfloat16)
    back_grad, gate_grad_out = (back_grad, gate_grad_out)
    return (fwd_out, back_grad, gate_grad_out)


MESH = pl.DeviceIdType.MESH


def wide_dot(a, b):
    return lax.dot_general(a, b, (((1,), (1,)), ((), ())), preferred_element_type=jnp.float32)


def layer_kernel(
    planes, plane, fwd_ref, tokens_ref, grad_ref, gain_ref, gate_ref, up_ref, down_ref, sum_ref,
    fwd_out, back_out, sum_out,
    turned, normed, toks, weights, fwd_gate, fwd_up, back_gate, back_up, hidden, gate_diff, up_diff,
    part, crossed, joined, gathered, grad_send, lifted, dropped, grad_recv, grad_cols,
    stage_sem, weight_sem, up_sem, down_sem, tok_send, tok_recv, relay_send, relay_recv,
    lift_send, lift_recv, drop_send, drop_recv, turn_send, turn_recv, cross_sem, join_send, join_recv, last_sem,
):
    n_fs = planes * plane
    fs, core = lax.axis_index("fs"), lax.axis_index("tp")
    level, place = fs // plane, fs % plane
    sibling = (fs, 1 - core)
    rows = weights.shape[1]
    depth = gate_ref.shape[0]
    half = fwd_ref.shape[0] // 2
    slab = half * plane
    width = fwd_ref.shape[1]

    barrier = pltpu.get_barrier_semaphore()
    for step in range(1, plane):
        to = level * plane + (place + step) % plane
        pl.semaphore_signal(barrier, inc=1, device_id=(to, core), device_id_type=MESH)
    for step in (1, planes - 1):
        to = (fs + step * plane) % n_fs
        pl.semaphore_signal(barrier, inc=1, device_id=(to, core), device_id_type=MESH)
    pl.semaphore_signal(barrier, inc=1, device_id=sibling, device_id_type=MESH)

    @pl.loop(0, turned.shape[1] // 128)
    def _(t):
        at = pl.ds(pl.multiple_of(t * 128, 128), 128)
        turned[0, at, :] = gate_ref[:, at].T
        turned[1, at, :] = up_ref[:, at].T
        turned[2, at, :] = down_ref[:, at].T

    @pl.loop(0, fwd_ref.shape[0] // 16)
    def _(r):
        at = pl.ds(pl.multiple_of(r * 16, 16), 16)
        for a, ref in ((0, tokens_ref), (1, fwd_ref)):
            normed[a, at, :] = normalize(ref[at, :], gain_ref[...])[2]

    pl.semaphore_wait(barrier, plane + 2)

    def remote(src, dst, send, recv, device):
        return pltpu.make_async_remote_copy(
            src_ref=src, dst_ref=dst, send_sem=send, recv_sem=recv, device_id=device, device_id_type=MESH
        )

    def own_block(w, q):
        return turned.at[w, pl.ds(pl.multiple_of(q * rows, rows), rows), :]

    def block(w, src):
        return weights.at[w, :, pl.ds(pl.multiple_of(src * depth, depth), depth)]

    def staged(w, step):
        q = (place + step) % plane
        return remote(own_block(w, q), block(w, fs), stage_sem.at[w, step], weight_sem.at[w, fs], (level * plane + q, core))

    def arrived(w, src):
        remote(block(w, src), block(w, src), stage_sem.at[w, 0], weight_sem.at[w, src], sibling).wait_recv()

    def hop(w, src, source, step):
        sem = up_sem if step > 0 else down_sem
        return remote(source, block(w, src), sem.at[w, src], weight_sem.at[w, src], ((fs + step * plane + n_fs) % n_fs, core))

    can = {1: level < planes - 1, -1: level > 0}

    def send_on(w, src, source, step):
        @pl.when(can[step])
        def _():
            hop(w, src, source, step).start()

    def token_rows(a, at):
        return grad_ref.at[at, :] if a == 2 else normed.at[a, at, :]

    def tok_block(a, h, q):
        return toks.at[a, h, pl.ds(pl.multiple_of(q * half, half), half), :]

    def tok_copy(a, step):
        q = (place + step) % plane
        return remote(
            token_rows(a, pl.ds(pl.multiple_of(core * half, half), half)),
            tok_block(a, core, place), tok_send.at[a, step], tok_recv.at[a, place], (level * plane + q, core),
        )

    def tok_arrived(a, q):
        remote(tok_block(a, core, q), tok_block(a, core, q), tok_send.at[a, 0], tok_recv.at[a, q], sibling).wait_recv()

    def relay(a, q):
        return remote(tok_block(a, core, q), tok_block(a, core, q), relay_send.at[a, q], relay_recv.at[a, q], sibling)

    def relayed(a, q):
        remote(tok_block(a, 1 - core, q), tok_block(a, 1 - core, q), relay_send.at[a, q], relay_recv.at[a, q], sibling).wait_recv()

    for w in range(3):
        for step in range(1, plane):
            staged(w, step).start()
        for step in (1, -1):
            send_on(w, fs, own_block(w, place), step)
    for a in range(3):
        for step in range(1, plane):
            tok_copy(a, step).start()
    for w in range(3):
        weights[w, :, pl.ds(pl.multiple_of(fs * depth, depth), depth)] = turned[w, pl.ds(pl.multiple_of(place * rows, rows), rows), :]
    for a in range(3):
        for h in range(2):
            toks[a, h, pl.ds(pl.multiple_of(place * half, half), half), :] = token_rows(a, pl.ds(h * half, half))[...]

    def group(w, d):
        if d == 0:
            for step in range(1, plane):
                src = level * plane + (place + step) % plane
                arrived(w, src)
                for way in (1, -1):
                    send_on(w, src, block(w, src), way)
            return
        for way in (1, -1):
            other = level - way * d

            @pl.when(jnp.logical_and(other >= 0, other < planes))
            def _():
                @pl.loop(0, plane)
                def _(q):
                    src = other * plane + q
                    arrived(w, src)
                    send_on(w, src, block(w, src), way)

    def relays(a):
        for step in range(1, plane):
            q = (place + step) % plane
            tok_arrived(a, q)
            relay(a, q).start()

    def relays_in(a):
        for step in range(1, plane):
            relayed(a, (place + step) % plane)

    def project(a, w, out):
        @pl.loop(0, 2)
        def _(h):
            out[h] = wide_dot(toks[a, h], weights[w])

    for d in range(planes - 1):
        for w in range(3):
            group(w, d)
    for a in range(3):
        relays(a)
    for a in range(3):
        relays_in(a)
    group(0, planes - 1)
    project(0, 0, back_gate)
    project(1, 0, fwd_gate)
    group(1, planes - 1)
    project(0, 1, back_up)
    project(1, 1, fwd_up)

    piece = 64

    @pl.loop(0, 2)
    def _(h):
        @pl.loop(0, slab // piece)
        def _(r):
            at = pl.ds(pl.multiple_of(r * piece, piece), piece)
            gate = fwd_gate[h, at, :]
            hidden[h, at, :] = (gate * jax.nn.sigmoid(gate) * fwd_up[h, at, :]).astype(jnp.bfloat16)
            gate = back_gate[h, at, :]
            s = jax.nn.sigmoid(gate)
            back_gate[h, at, :] = gate * s
            back_up[h, at, :] = back_up[h, at, :] * s * (1.0 + gate * (1.0 - s))

    group(2, planes - 1)

    @pl.loop(0, 2)
    def _(h):
        back = 0.5 * wide_dot(toks[2, h], weights[2])
        fwd_gate[h] = back
        gate_diff[pl.ds(pl.multiple_of(h * slab, slab), slab), :] = (back * back_up[h]).astype(jnp.bfloat16)
        up_diff[pl.ds(pl.multiple_of(h * slab, slab), slab), :] = (back * back_gate[h]).astype(jnp.bfloat16)

    def grad_hop(b, way):
        sends, recvs, lands = (lift_send, lift_recv, lifted) if way > 0 else (drop_send, drop_recv, dropped)
        to = (fs + way * plane + n_fs) % n_fs
        return remote(grad_send.at[b], lands.at[b], sends.at[b], recvs.at[b], (to, core))

    diff_turned = gate_diff[...].T

    for step in range(planes):
        there = jnp.where(2 * level < planes, planes - 1 - step, step)
        cols = pl.ds(pl.multiple_of(there * plane * depth, plane * depth), plane * depth)
        product = jnp.dot(diff_turned[:, :slab], toks[0, 0, :, cols], preferred_element_type=jnp.float32)
        product = product + jnp.dot(diff_turned[:, slab:], toks[0, 1, :, cols], preferred_element_type=jnp.float32)
        product = product.astype(jnp.bfloat16)
        for q in range(plane):
            grad_send[there * plane + q] = product[:, q * depth : (q + 1) * depth]
        for way, first in ((1, 0), (-1, planes - 1)):

            @pl.when(jnp.logical_and(level == first, there != first))
            def _():
                for q in range(plane):
                    grad_hop(there * plane + q, way).start()

    def serve(i):
        for way in (1, -1):
            lands = lifted if way > 0 else dropped
            there = planes - 1 - i if way > 0 else i
            left = (there - level) * way

            @pl.when(jnp.logical_and(can[-way], left >= 0))
            def _():
                @pl.loop(0, plane)
                def _(q):
                    b = there * plane + q
                    grad_hop(b, way).wait_recv()
                    total = grad_send[b].astype(jnp.float32) + lands[b].astype(jnp.float32)
                    grad_send[b] = total.astype(jnp.bfloat16)

                    @pl.when(left > 0)
                    def _():
                        grad_hop(b, way).start()

    def turn(step):
        q = (place + step) % plane
        return remote(grad_send.at[level * plane + q], grad_recv.at[place], turn_send.at[step], turn_recv.at[place], (level * plane + q, core))

    def cross(k):
        return remote(part.at[k, 1 - core], crossed.at[k], cross_sem.at[k, 0], cross_sem.at[k, 1], sibling)

    def join(k, step):
        q = (place + step) % plane
        return remote(joined.at[k, q], gathered.at[k, place], join_send.at[k, step], join_recv.at[k, place], (level * plane + q, core))

    strip = 512

    def partial(k, h):
        rows_at = pl.ds(pl.multiple_of(h * slab, slab), slab)

        @pl.loop(0, width // strip)
        def _(t):
            at = pl.ds(pl.multiple_of(t * strip, strip), strip)
            if k == 0:
                value = jnp.dot(hidden[h], weights[2, :, at], preferred_element_type=jnp.float32)
            else:
                value = jnp.dot(gate_diff[rows_at, :], weights[0, :, at], preferred_element_type=jnp.float32)
                value = value + jnp.dot(up_diff[rows_at, :], weights[1, :, at], preferred_element_type=jnp.float32)
            part[k, h, :, at] = value.astype(jnp.bfloat16)

    for k in range(2):
        partial(k, 1 - core)
        cross(k).start()
    for k in range(2):
        partial(k, core)
    for k in range(2):
        cross(k).wait_recv()
        for step in range(plane):
            q = (place + step + 1) % plane
            at = pl.ds(pl.multiple_of(q * half, half), half)
            total = part[k, core, at, :].astype(jnp.float32) + crossed[k, at, :].astype(jnp.float32)
            joined[k, q] = total.astype(jnp.bfloat16)
            if step < plane - 1:
                join(k, step + 1).start()
    for i in range(planes):
        serve(i)
    for step in range(1, plane):
        turn(step).start()
    grad_recv[place] = grad_send[fs]
    for k in range(2):
        gathered[k, place] = joined[k, place]

    mine = pl.ds(pl.multiple_of(core * half, half), half)

    def last(k):
        out = (fwd_out, back_out)[k]
        return remote(out.at[mine, :], out.at[mine, :], last_sem.at[k, 0], last_sem.at[k, 1], sibling)

    def joined_in(k):
        for step in range(1, plane):
            q = (place + step) % plane
            remote(joined.at[k, q], gathered.at[k, q], join_send.at[k, 0], join_recv.at[k, q], sibling).wait_recv()

    def total_of(k, at):
        value = gathered[k, 0, at, :].astype(jnp.float32)
        for q in range(1, plane):
            value = value + gathered[k, q, at, :].astype(jnp.float32)
        return value

    small = 16
    joined_in(0)
    for r in range(half // small):
        at = pl.ds(r * small, small)
        fwd_out[pl.ds(pl.multiple_of(core * half + r * small, small), small), :] = (0.5 * total_of(0, at)).astype(jnp.bfloat16)
    joined_in(1)
    for r in range(half // small):
        at = pl.ds(r * small, small)
        there = pl.ds(pl.multiple_of(core * half + r * small, small), small)
        values = tokens_ref[there, :].astype(jnp.float32)
        factor = lax.rsqrt(jnp.mean(values * values, axis=-1, keepdims=True) + norm_eps)
        scaled = total_of(1, at) * gain_ref[...]
        cubed = factor * factor * factor
        back_out[there, :] = (
            factor * scaled - values * cubed * jnp.mean(scaled * values, axis=-1, keepdims=True)
        ).astype(jnp.bfloat16)
    for k in range(2):
        last(k).start()

    for step in range(1, plane):
        q = (place + step) % plane
        remote(grad_send.at[fs], grad_recv.at[q], turn_send.at[0], turn_recv.at[q], sibling).wait_recv()
    for q in range(plane):
        grad_cols[q * rows : (q + 1) * rows, :] = grad_recv[q].astype(jnp.float32)

    @pl.loop(0, grad_cols.shape[0] // 128)
    def _(t):
        at = pl.ds(pl.multiple_of(t * 128, 128), 128)
        sum_out[:, at] = sum_ref[:, at] + grad_cols[at, :].T

    for w in range(3):
        for step in range(1, plane):
            staged(w, step).wait_send()
        for way in (1, -1):
            for d in range(planes - 1):
                other = level - way * d

                @pl.when(jnp.logical_and(can[way], jnp.logical_and(other >= 0, other < planes)))
                def _():
                    @pl.loop(0, plane)
                    def _(q):
                        src = other * plane + q
                        hop(w, src, block(w, src), way).wait_send()

    for a in range(3):
        for step in range(1, plane):
            tok_copy(a, step).wait_send()
            relay(a, (place + step) % plane).wait_send()
    for step in range(1, plane):
        turn(step).wait_send()
    for way in (1, -1):

        @pl.when(can[way])
        def _():
            @pl.loop(0, planes)
            def _(there):
                @pl.when((there - level) * way > 0)
                def _():
                    @pl.loop(0, plane)
                    def _(q):
                        grad_hop(there * plane + q, way).wait_send()

    for k in range(2):
        cross(k).wait_send()
        for step in range(1, plane):
            join(k, step).wait_send()
        last(k).wait()


def fused_shards(
    planes, plane, fwd_tokens, back_tokens, out_grad, norm_gain, gate_weight, up_weight, down_weight, gate_grad_sum
):
    tokens, width = fwd_tokens.shape
    depth, cols = gate_weight.shape
    rows = cols // plane
    half = tokens // 2
    slab = half * plane
    n_fs = planes * plane
    narrow, full = jnp.bfloat16, jnp.float32
    dma = pltpu.SemaphoreType.DMA
    vmem = pl.BlockSpec(memory_space=pltpu.VMEM)
    return pl.pallas_call(
        functools.partial(layer_kernel, planes, plane),
        out_shape=(
            jax.ShapeDtypeStruct((tokens, width), narrow),
            jax.ShapeDtypeStruct((tokens, width), narrow),
            jax.ShapeDtypeStruct((depth, cols), full),
        ),
        in_specs=[vmem] * 8,
        out_specs=(vmem,) * 3,
        scratch_shapes=[
            pltpu.VMEM((3, cols, depth), narrow),
            pltpu.VMEM((2, tokens, width), narrow),
            pltpu.VMEM((3, 2, slab, width), narrow),
            pltpu.VMEM((3, rows, width), narrow),
            pltpu.VMEM((2, slab, rows), full),
            pltpu.VMEM((2, slab, rows), full),
            pltpu.VMEM((2, slab, rows), full),
            pltpu.VMEM((2, slab, rows), full),
            pltpu.VMEM((2, slab, rows), narrow),
            pltpu.VMEM((2 * slab, rows), narrow),
            pltpu.VMEM((2 * slab, rows), narrow),
            pltpu.VMEM((2, 2, slab, width), narrow),
            pltpu.VMEM((2, slab, width), narrow),
            pltpu.VMEM((2, plane, half, width), narrow),
            pltpu.VMEM((2, plane, half, width), narrow),
            pltpu.VMEM((n_fs, rows, depth), narrow),
            pltpu.VMEM((n_fs, rows, depth), narrow),
            pltpu.VMEM((n_fs, rows, depth), narrow),
            pltpu.VMEM((plane, rows, depth), narrow),
            pltpu.VMEM((cols, depth), full),
            dma((3, plane)),
            dma((3, n_fs)),
            dma((3, n_fs)),
            dma((3, n_fs)),
            dma((3, plane)),
            dma((3, plane)),
            dma((3, plane)),
            dma((3, plane)),
            dma((n_fs,)),
            dma((n_fs,)),
            dma((n_fs,)),
            dma((n_fs,)),
            dma((plane,)),
            dma((plane,)),
            dma((2, 2)),
            dma((2, plane)),
            dma((2, plane)),
            dma((2, 2)),
        ],
        compiler_params=pltpu.CompilerParams(
            collective_id=0, has_side_effects=True, vmem_limit_bytes=56 * 2**20
        ),
    )(
        fwd_tokens, back_tokens, out_grad, norm_gain.reshape(1, width),
        gate_weight, up_weight, down_weight, gate_grad_sum,
    )


def square_side(count):
    side = 1
    while side * side * 4 <= count:
        side *= 2
    return side


def body_for(mesh):
    n_fs, plane = mesh.shape["fs"], square_side(mesh.shape["fs"])

    def body(*args):
        tokens, width = args[0].shape
        depth, cols = args[4].shape
        fits = (
            mesh.shape["tp"] == 2 and n_fs % plane == 0 and n_fs // plane >= 3 and plane >= 2
            and depth == 128 and cols % (plane * 16) == 0 and cols % 128 == 0
            and tokens % 128 == 0 and width % 512 == 0
        )
        if not fits:
            return shards(*args)
        return fused_shards(n_fs // plane, plane, *args)

    return body


def solution(mesh):
    in_specs = (
        P("fs", None),
        P("fs", None),
        P("fs", None),
        P(),
        P("fs", "tp"),
        P("fs", "tp"),
        P("fs", "tp"),
        P("fs", "tp"),
    )
    out_specs = (P("fs", None), P("fs", None), P("fs", "tp"))
    return jax.shard_map(body_for(mesh), mesh=mesh, in_specs=in_specs, out_specs=out_specs, check_vma=False)
```

profile of v0, /device:TPU:0, one launch (start us, length us, event | category | flops | bytes accessed | tf_op | source)
XLA Modules:
  0.0 123.9 jit_solution(12393041260954732137)
XLA Ops:
  0.6 119.2 %shard_map.103 = (bf16[128,2048]{1,0:T(8,128)(2,1)}, bf16[128,2048]{1,0:T(8,128)(2,1)}, f32[128,1408]{1,0:T(8,128)}) custom-call(bf16[128,2048]{1,0:T(8,128)(2,1)} %fwd_ref.1, bf16[128,2048]{1,0:T(8,128)(2,1)} %tokens_ref.1, bf16[128,2048]{1,0:T(8,128)(2,1)} %grad_ref.1, f32[1,2048]{1,0:T(1,128)} %bitcast.1, bf16[128,1408]{1,0:T(8,128)(2,1)} %gate_ref.1, ...), custom_call_target="tpu_custom_call" | custom-call | tf_op jit(solution)/shard_map/pallas_call | solution.py:445
  119.8 0.0 copy-start.1
  119.8 1.9 %copy.14 = bf16[128,2048]{1,0:T(8,128)(2,1)} copy(bf16[128,2048]{1,0:T(8,128)(2,1)} %get-tuple-element.6) | data formatting | bytes 1048576
  121.7 0.0 copy-done.1
  121.7 0.0 copy-start
  121.7 0.8 copy.15
  122.5 0.5 copy-done
  123.0 0.9 copy.16
Async XLA Ops:
  119.8 2.0 %copy-start.1 = (bf16[128,2048]{1,0:T(8,128)(2,1)S(1)}, bf16[128,2048]{1,0:T(8,128)(2,1)}, u32[]{:S(2)}) copy-start(bf16[128,2048]{1,0:T(8,128)(2,1)} %get-tuple-element.7) | copy-start | bytes 1572868
  121.7 1.3 %copy-start = (f32[128,1408]{1,0:T(8,128)S(1)}, f32[128,1408]{1,0:T(8,128)}, u32[]{:S(2)}) copy-start(f32[128,1408]{1,0:T(8,128)} %get-tuple-element.8) | copy-start | bytes 2162692
where the time goes:
time: 126 us; the launch traced here: 124 us
  Pallas kernels  119 us (94%)
  local copies, waits for them, and re-layouts  4.1 us (3%)
    pallas_call x1, Pallas kernels, fused_shards(): pl.pallas_call(functools.partial(layer_kernel, planes, plane), out_shape=...  119 us
    unnamed x7, local copies, waits for them, and re-layouts  4.1 us

commit v1 on v0

v1 whole, which is shorter than its diff:
```python
import functools

import jax
import jax.numpy as jnp
from jax import lax
from jax.experimental import pallas as pl
from jax.experimental.pallas import tpu as pltpu
from jax.sharding import PartitionSpec as P

norm_eps = 0.25


def normalize(tokens, norm_gain):
    values = tokens.astype(jnp.float32)
    factor = lax.rsqrt(jnp.mean(values * values, axis=-1, keepdims=True) + norm_eps)
    return (values, factor, (values * factor * norm_gain).astype(jnp.bfloat16))


def shards(
    fwd_tokens, back_tokens, out_grad, norm_gain, gate_weight, up_weight, down_weight, gate_grad_sum
):
    fwd_normed = normalize(fwd_tokens, norm_gain)[2]
    columns = fwd_normed
    gate_pre = jnp.dot(
        columns,
        lax.all_gather(gate_weight, "fs", axis=0, tiled=True),
        preferred_element_type=jnp.float32,
    )
    up_pre = jnp.dot(
        columns,
        lax.all_gather(up_weight, "fs", axis=0, tiled=True),
        preferred_element_type=jnp.float32,
    )
    hidden = (gate_pre * jax.nn.sigmoid(gate_pre) * up_pre).astype(jnp.bfloat16)
    partial_value = jnp.dot(
        hidden,
        lax.all_gather(down_weight, "fs", axis=0, tiled=True).T,
        preferred_element_type=jnp.float32,
    )
    summed = lax.psum(partial_value.astype(jnp.bfloat16), "tp").astype(jnp.float32)
    fwd_out = (0.5 * summed).astype(jnp.bfloat16)
    gate_whole = lax.all_gather(gate_weight, "fs", axis=0, tiled=True)
    up_whole = lax.all_gather(up_weight, "fs", axis=0, tiled=True)
    down_whole = lax.all_gather(down_weight, "fs", axis=0, tiled=True)
    values, factor, back_normed = normalize(back_tokens, norm_gain)
    gate_pre = jnp.dot(back_normed, gate_whole, preferred_element_type=jnp.float32)
    up_pre = jnp.dot(back_normed, up_whole, preferred_element_type=jnp.float32)
    sigmoid_gate = jax.nn.sigmoid(gate_pre)
    back_hidden = 0.5 * jnp.dot(out_grad, down_whole, preferred_element_type=jnp.float32)
    gate_diff = (
        back_hidden * up_pre * sigmoid_gate * (1.0 + gate_pre * (1.0 - sigmoid_gate))
    ).astype(jnp.bfloat16)
    up_diff = (back_hidden * gate_pre * sigmoid_gate).astype(jnp.bfloat16)
    columns = back_normed
    gate_grad_out = gate_grad_sum + lax.psum_scatter(
        jnp.dot(columns.T, gate_diff, preferred_element_type=jnp.float32),
        "fs",
        scatter_dimension=0,
        tiled=True,
    )
    partial_diff = jnp.dot(gate_diff, gate_whole.T, preferred_element_type=jnp.float32)
    partial_diff = partial_diff + jnp.dot(up_diff, up_whole.T, preferred_element_type=jnp.float32)
    normed_diff = lax.psum(partial_diff.astype(jnp.bfloat16), "tp").astype(jnp.float32)
    scaled = normed_diff * norm_gain
    cubed = factor * factor * factor
    back_grad = (
        factor * scaled - values * cubed * jnp.mean(scaled * values, axis=-1, keepdims=True)
    ).astype(jnp.bfloat16)
    back_grad, gate_grad_out = (back_grad, gate_grad_out)
    return (fwd_out, back_grad, gate_grad_out)


MESH = pl.DeviceIdType.MESH


def wide_dot(a, b):
    return lax.dot_general(a, b, (((1,), (1,)), ((), ())), preferred_element_type=jnp.float32)


def layer_kernel(
    parts, fwd_ref, tokens_ref, grad_ref, gain_ref, gate_ref, up_ref, down_ref, sum_ref,
    fwd_out, back_out, sum_out,
    turned, normed, toks, weights, staged, acc, hidden, gate_diff, up_diff,
    part, crossed, joined, folded, gathered, grad_send, grad_side, grad_total, grad_recv, grad_cols,
    stage_send, stage_recv, weight_recv, far_send, near_send, other_send, pass_send, side_send,
    tok_send, tok_recv, relay_send, relay_recv, gside_send, gside_recv, gdir_send, gdir_recv,
    cross_sem, join_send, join_recv, last_sem,
):
    fs, core = lax.axis_index("fs"), lax.axis_index("tp")
    x, y, z = fs % 2, fs // 2 % 2, fs // 4
    odd = z % 2
    inner = jnp.logical_and(z > 0, z < 3)
    near, far, other = z + 1 - 2 * odd, (z + 2) % 4, 3 - z
    sibling = (fs, 1 - core)
    rows = weights.shape[2]
    depth = gate_ref.shape[0]
    half = fwd_ref.shape[0] // 2
    slab = half * 4
    width = fwd_ref.shape[1]
    band = 4 * depth

    def chip(to_x, to_y, to_z):
        return (to_z * 4 + to_y * 2 + to_x, core)

    beside, across = chip(1 - x, y, z), chip(x, 1 - y, z)

    barrier = pltpu.get_barrier_semaphore()
    for device in (
        sibling, beside, across, chip(x, y, near), chip(x, y, far), chip(x, y, other),
        chip(x, 1 - y, near), chip(x, 1 - y, far), chip(x, 1 - y, other),
    ):
        pl.semaphore_signal(barrier, inc=1, device_id=device, device_id_type=MESH)

    @pl.loop(0, turned.shape[1] // 128)
    def _(t):
        at = pl.ds(pl.multiple_of(t * 128, 128), 128)
        turned[0, at, :] = gate_ref[:, at].T
        turned[1, at, :] = up_ref[:, at].T
        turned[2, at, :] = down_ref[:, at].T

    pl.semaphore_wait(barrier, 9)

    def remote(src, dst, send, recv, device):
        return pltpu.make_async_remote_copy(
            src_ref=src, dst_ref=dst, send_sem=send, recv_sem=recv, device_id=device, device_id_type=MESH
        )

    def own_rows(h, to_y, to_odd):
        return pl.ds(pl.multiple_of(((to_y * 2 + to_odd) * parts + h) * rows, 16), rows)

    def own(w, h, to_y, to_odd):
        return turned.at[w, own_rows(h, to_y, to_odd), :]

    def lanes(src):
        return pl.ds(pl.multiple_of(src * depth, depth), depth)

    def level_lanes(s):
        return pl.ds(pl.multiple_of(s * band, band), band)

    def block(w, h, src):
        return weights.at[w, h, :, lanes(src)]

    def send_block(w, h, src, source, sem, device):
        return remote(source, block(w, h, src), sem, weight_recv.at[w, h, src], device)

    def block_in(w, h, src):
        send_block(w, h, src, block(w, h, src), stage_send.at[w, h, 0], sibling).wait_recv()

    def side(w, h, src, source):
        return send_block(w, h, src, source, side_send.at[w, h, src // 2], beside)

    def held(w, h):
        return remote(own(w, h, 1 - y, 1 - odd), staged.at[w, h], stage_send.at[w, h, 1], stage_recv.at[w, h], across)

    def send_own(h):
        for w in range(3):
            send_block(w, h, fs, own(w, h, 1 - y, odd), stage_send.at[w, h, 0], across).start()
            held(w, h).start()
            send_block(w, h, fs, own(w, h, y, 1 - odd), near_send.at[w, h, 0], chip(x, y, near)).start()
            send_block(w, h, fs, own(w, h, y, odd), far_send.at[w, h, 0], chip(x, y, far)).start()

            @pl.when(inner)
            def _():
                send_block(w, h, fs, own(w, h, y, 1 - odd), other_send.at[w, h, 0], chip(x, y, other)).start()

            side(w, h, fs, own(w, h, y, odd)).start()

    def keep_own(h):
        for w in range(3):
            weights[w, h, :, lanes(fs)] = turned[w, own_rows(h, y, odd), :]

    def stage_in(w, h):
        src = z * 4 + (1 - y) * 2 + x
        held(w, h).wait_recv()
        send_block(w, h, src, staged.at[w, h], near_send.at[w, h, 1], chip(x, y, near)).start()

        @pl.when(inner)
        def _():
            send_block(w, h, src, staged.at[w, h], other_send.at[w, h, 1], chip(x, y, other)).start()

        block_in(w, h, src)
        send_block(w, h, src, block(w, h, src), far_send.at[w, h, 1], chip(x, y, far)).start()
        side(w, h, src, block(w, h, src)).start()

    def level_in(w, h, s, passed):
        for line in range(2):
            src = s * 4 + line * 2 + x
            block_in(w, h, src)
            if passed:

                @pl.when(inner)
                def _():
                    send_block(w, h, src, block(w, h, src), pass_send.at[w, h, line], chip(x, y, far)).start()

            side(w, h, src, block(w, h, src)).start()

    def side_in(w, h, s):
        for line in range(2):
            block_in(w, h, s * 4 + line * 2 + 1 - x)

    me = y * 2 + odd
    at_near, at_across, at_both = y * 2 + 1 - odd, (1 - y) * 2 + odd, (1 - y) * 2 + 1 - odd

    def token_rows(a, at):
        return grad_ref.at[at, :] if a == 2 else normed.at[a, at, :]

    def tok_block(a, h, q):
        return toks.at[a, h, pl.ds(pl.multiple_of(q * half, half), half), :]

    def tok_copy(a, n, q, source, device):
        return remote(source, tok_block(a, core, q), tok_send.at[a, n], tok_recv.at[a, q], device)

    def relay(a, q):
        return remote(tok_block(a, core, q), tok_block(a, core, q), relay_send.at[a, q], relay_recv.at[a, q], sibling)

    def send_tokens(a):
        mine = token_rows(a, pl.ds(pl.multiple_of(core * half, half), half))
        tok_copy(a, 0, me, mine, chip(x, y, near)).start()
        tok_copy(a, 1, me, mine, across).start()

    def keep_tokens(a):
        for h in range(2):
            toks[a, h, pl.ds(pl.multiple_of(me * half, half), half), :] = token_rows(a, pl.ds(h * half, half))[...]

    def tok_in(a, q):
        tok_copy(a, 0, q, tok_block(a, core, q), sibling).wait_recv()
        if q is at_near:
            tok_copy(a, 2, q, tok_block(a, core, q), across).start()
        relay(a, q).start()

    def relayed(a):
        for q in (at_near, at_across, at_both):
            remote(tok_block(a, 1 - core, q), tok_block(a, 1 - core, q), relay_send.at[a, q], relay_recv.at[a, q], sibling).wait_recv()

    def project(h, s, pairs, first):
        at = level_lanes(s)
        for i, a, w in pairs:

            @pl.loop(0, 2)
            def _(t):
                value = wide_dot(toks[a, t, :, at], weights[w, h, :, at])
                acc[i, h, t] = value if first else acc[i, h, t] + value

    back_pairs = ((0, 0, 0), (1, 0, 1), (2, 2, 2))
    fwd_pairs = ((3, 1, 0), (4, 1, 1))
    piece = 64

    def back_parts(h):
        @pl.loop(0, 2)
        def _(t):
            @pl.loop(0, slab // piece)
            def _(r):
                at = pl.ds(pl.multiple_of(r * piece, piece), piece)
                gate = acc[0, h, t, at, :]
                s = jax.nn.sigmoid(gate)
                back = 0.5 * acc[2, h, t, at, :]
                there = pl.ds(pl.multiple_of(t * slab + r * piece, piece), piece)
                gate_diff[h, there, :] = (back * acc[1, h, t, at, :] * s * (1.0 + gate * (1.0 - s))).astype(jnp.bfloat16)
                up_diff[h, there, :] = (back * gate * s).astype(jnp.bfloat16)

    def fwd_parts(h):
        @pl.loop(0, 2)
        def _(t):
            @pl.loop(0, slab // piece)
            def _(r):
                at = pl.ds(pl.multiple_of(r * piece, piece), piece)
                gate = acc[3, h, t, at, :]
                hidden[h, t, at, :] = (gate * jax.nn.sigmoid(gate) * acc[4, h, t, at, :]).astype(jnp.bfloat16)

    def grad_across(h, s):
        pair = pl.ds(s * 2, 2)
        return remote(grad_send.at[h, 1 - x, pair], grad_side.at[h, pair], gside_send.at[h, s], gside_recv.at[h, s], beside)

    def grad_out(h):
        diff_turned = gate_diff[h].T
        for s in range(4):
            at = level_lanes(s)
            product = jnp.dot(diff_turned[:, :slab], toks[0, 0, :, at], preferred_element_type=jnp.float32)
            product = product + jnp.dot(diff_turned[:, slab:], toks[0, 1, :, at], preferred_element_type=jnp.float32)
            product = product.astype(jnp.bfloat16)
            for q in range(4):
                grad_send[h, q % 2, s * 2 + q // 2] = product[:, q * depth : (q + 1) * depth]
            grad_across(h, s).start()

    place = z * 2 + y

    def grad_direct(h, to_z, to_y):
        j = to_z * 2 + to_y
        return remote(grad_total.at[h, j], grad_recv.at[h, place], gdir_send.at[h, j], gdir_recv.at[h, place], chip(x, to_y, to_z))

    def each_direct(h, to_z, run):
        for to_y in range(2):

            @pl.when(jnp.logical_or(to_z != z, to_y != y))
            def _():
                run(grad_direct(h, to_z, to_y))

    def grad_on(h):
        for s in range(4):
            grad_across(h, s).wait_recv()
            for j in (s * 2, s * 2 + 1):
                total = grad_send[h, x, j].astype(jnp.float32) + grad_side[h, j].astype(jnp.float32)
                grad_total[h, j] = total.astype(jnp.bfloat16)
            each_direct(h, s, lambda copy: copy.start())
        grad_recv[h, place] = grad_total[h, place]

    def grad_in(h):
        for s in range(4):
            for line in range(2):
                j = s * 2 + line

                @pl.when(j != place)
                def _():
                    remote(grad_recv.at[h, j], grad_recv.at[h, j], gdir_send.at[h, j], gdir_recv.at[h, j], sibling).wait_recv()
        for line in range(2):
            for s in range(2):
                total = grad_recv[h, s * 2 + line].astype(jnp.float32) + grad_recv[h, s * 2 + 4 + line].astype(jnp.float32)
                first = ((line * 2 + s) * parts + h) * rows
                grad_cols[first : first + rows, :] = total

    def cross(k):
        return remote(part.at[k, 1 - core], crossed.at[k], cross_sem.at[k, 0], cross_sem.at[k, 1], sibling)

    strip = 512

    def partial(k, t):
        rows_at = pl.ds(pl.multiple_of(t * slab, slab), slab)

        @pl.loop(0, width // strip)
        def _(c):
            at = pl.ds(pl.multiple_of(c * strip, strip), strip)
            value = 0.0
            for h in range(parts):
                if k == 0:
                    value = value + jnp.dot(hidden[h, t], weights[2, h, :, at], preferred_element_type=jnp.float32)
                else:
                    value = value + jnp.dot(gate_diff[h, rows_at, :], weights[0, h, :, at], preferred_element_type=jnp.float32)
                    value = value + jnp.dot(up_diff[h, rows_at, :], weights[1, h, :, at], preferred_element_type=jnp.float32)
            part[k, t, :, at] = value.astype(jnp.bfloat16)

    firsts = ((across, at_across, at_near), (chip(x, y, near), at_near, at_across))
    seconds = (chip(x, y, near), across)

    def join_copy(k, n):
        to, theirs, mine = firsts[k]
        if n == 2:
            return remote(folded.at[k], gathered.at[k, 2], join_send.at[k, 2], join_recv.at[k, 2], seconds[k])
        return remote(joined.at[k, (at_both, theirs)[n]], gathered.at[k, n], join_send.at[k, n], join_recv.at[k, n], to)

    def join_start(k):
        cross(k).wait_recv()
        for n, q in enumerate((at_both, firsts[k][1], firsts[k][2], me)):
            at = pl.ds(pl.multiple_of(q * half, half), half)
            total = part[k, core, at, :].astype(jnp.float32) + crossed[k, at, :].astype(jnp.float32)
            joined[k, q] = total.astype(jnp.bfloat16)
            if n < 2:
                join_copy(k, n).start()

    def join_fold(k):
        join_copy(k, 0).wait_recv()
        total = gathered[k, 0].astype(jnp.float32) + joined[k, firsts[k][2]].astype(jnp.float32)
        folded[k] = total.astype(jnp.bfloat16)
        join_copy(k, 2).start()

    send_own(0)
    for a in (0, 1):

        @pl.loop(0, tokens_ref.shape[0] // 16)
        def _(r):
            at = pl.ds(pl.multiple_of(r * 16, 16), 16)
            normed[a, at, :] = normalize((tokens_ref, fwd_ref)[a][at, :], gain_ref[...])[2]

        if a == 0:
            send_tokens(2)
            send_tokens(0)
    for h in range(parts):
        keep_own(h)
    for a in range(3):
        keep_tokens(a)
    for w in range(3):
        stage_in(w, 0)
    for w in range(3):
        level_in(w, 0, near, True)
    if parts > 1:
        send_own(1)
    send_tokens(1)
    for w in range(3):
        level_in(w, 0, far, False)
    for a in (2, 0):
        tok_in(a, at_across)
        tok_in(a, at_near)
    for w in range(3):
        level_in(w, 0, other, False)
    if parts > 1:
        for w in range(3):
            stage_in(w, 1)
    for a in (2, 0):
        tok_in(a, at_both)
        relayed(a)
    for w in range(3):
        side_in(w, 0, z)
    project(0, z, back_pairs, True)
    if parts > 1:
        for w in range(3):
            level_in(w, 1, near, True)
    for w in range(3):
        side_in(w, 0, near)
    project(0, near, back_pairs, False)
    if parts > 1:
        for w in range(3):
            level_in(w, 1, far, False)
    for w in range(3):
        side_in(w, 0, far)
    project(0, far, back_pairs, False)
    for w in range(3):
        side_in(w, 0, other)
    project(0, other, back_pairs, False)
    back_parts(0)
    grad_out(0)
    tok_in(1, at_across)
    tok_in(1, at_near)
    if parts > 1:
        for w in range(3):
            level_in(w, 1, other, False)
    tok_in(1, at_both)
    relayed(1)
    for n, s in enumerate((z, near, far, other)):
        project(0, s, fwd_pairs, n == 0)
    fwd_parts(0)
    grad_on(0)
    if parts > 1:
        for n, s in enumerate((z, near, far, other)):
            for w in range(3):
                side_in(w, 1, s)
            project(1, s, fwd_pairs + back_pairs, n == 0)
        fwd_parts(1)
    partial(0, 1 - core)
    cross(0).start()
    if parts > 1:
        back_parts(1)
    partial(1, 1 - core)
    cross(1).start()
    partial(0, core)
    join_start(0)
    partial(1, core)
    join_start(1)
    if parts > 1:
        grad_out(1)
    join_fold(0)
    join_fold(1)
    if parts > 1:
        grad_on(1)

    mine = pl.ds(pl.multiple_of(core * half, half), half)

    def last(k):
        out = (fwd_out, back_out)[k]
        return remote(out.at[mine, :], out.at[mine, :], last_sem.at[k, 0], last_sem.at[k, 1], sibling)

    def joined_in(k):
        for n in (1, 2):
            join_copy(k, n).wait_recv()

    def total_of(k, at):
        value = joined[k, me, at, :].astype(jnp.float32) + gathered[k, 1, at, :].astype(jnp.float32)
        return value + gathered[k, 2, at, :].astype(jnp.float32)

    small = 16
    joined_in(0)
    for r in range(half // small):
        at = pl.ds(r * small, small)
        fwd_out[pl.ds(pl.multiple_of(core * half + r * small, small), small), :] = (0.5 * total_of(0, at)).astype(jnp.bfloat16)
    last(0).start()
    joined_in(1)
    for r in range(half // small):
        at = pl.ds(r * small, small)
        there = pl.ds(pl.multiple_of(core * half + r * small, small), small)
        values = tokens_ref[there, :].astype(jnp.float32)
        factor = lax.rsqrt(jnp.mean(values * values, axis=-1, keepdims=True) + norm_eps)
        scaled = total_of(1, at) * gain_ref[...]
        cubed = factor * factor * factor
        back_out[there, :] = (
            factor * scaled - values * cubed * jnp.mean(scaled * values, axis=-1, keepdims=True)
        ).astype(jnp.bfloat16)
    last(1).start()

    for h in range(parts):
        grad_in(h)

    @pl.loop(0, grad_cols.shape[0] // 128)
    def _(t):
        at = pl.ds(pl.multiple_of(t * 128, 128), 128)
        sum_out[:, at] = sum_ref[:, at] + grad_cols[at, :].T

    for h in range(parts):
        for w in range(3):
            for n in range(2):
                gone = block(w, h, fs)
                for sem in (stage_send, near_send, far_send):
                    send_block(w, h, fs, gone, sem.at[w, h, n], sibling).wait_send()

                @pl.when(inner)
                def _():
                    for sem in (other_send, pass_send):
                        send_block(w, h, fs, gone, sem.at[w, h, n], sibling).wait_send()

            @pl.loop(0, 8)
            def _(j):
                send_block(w, h, fs, gone, side_send.at[w, h, j], sibling).wait_send()

        for s in range(4):
            grad_across(h, s).wait_send()
            each_direct(h, s, lambda copy: copy.wait_send())
    for a in range(3):
        for n in range(3):
            tok_copy(a, n, me, tok_block(a, core, me), sibling).wait_send()
        for q in (at_near, at_across, at_both):
            relay(a, q).wait_send()
    for k in range(2):
        cross(k).wait_send()
        for n in range(3):
            join_copy(k, n).wait_send()
        last(k).wait()


def fused_shards(
    parts, fwd_tokens, back_tokens, out_grad, norm_gain, gate_weight, up_weight, down_weight, gate_grad_sum
):
    tokens, width = fwd_tokens.shape
    depth, cols = gate_weight.shape
    rows = cols // (4 * parts)
    half = tokens // 2
    slab = half * 4
    narrow, full = jnp.bfloat16, jnp.float32
    dma = pltpu.SemaphoreType.DMA
    vmem = pl.BlockSpec(memory_space=pltpu.VMEM)
    return pl.pallas_call(
        functools.partial(layer_kernel, parts),
        out_shape=(
            jax.ShapeDtypeStruct((tokens, width), narrow),
            jax.ShapeDtypeStruct((tokens, width), narrow),
            jax.ShapeDtypeStruct((depth, cols), full),
        ),
        in_specs=[vmem] * 8,
        out_specs=(vmem,) * 3,
        scratch_shapes=[
            pltpu.VMEM((3, cols, depth), narrow),
            pltpu.VMEM((2, tokens, width), narrow),
            pltpu.VMEM((3, 2, slab, width), narrow),
            pltpu.VMEM((3, parts, rows, width), narrow),
            pltpu.VMEM((3, parts, rows, depth), narrow),
            pltpu.VMEM((5, parts, 2, slab, rows), full),
            pltpu.VMEM((parts, 2, slab, rows), narrow),
            pltpu.VMEM((parts, 2 * slab, rows), narrow),
            pltpu.VMEM((parts, 2 * slab, rows), narrow),
            pltpu.VMEM((2, 2, slab, width), narrow),
            pltpu.VMEM((2, slab, width), narrow),
            pltpu.VMEM((2, 4, half, width), narrow),
            pltpu.VMEM((2, half, width), narrow),
            pltpu.VMEM((2, 3, half, width), narrow),
            pltpu.VMEM((parts, 2, 8, rows, depth), narrow),
            pltpu.VMEM((parts, 8, rows, depth), narrow),
            pltpu.VMEM((parts, 8, rows, depth), narrow),
            pltpu.VMEM((parts, 8, rows, depth), narrow),
            pltpu.VMEM((cols, depth), full),
            dma((3, parts, 2)),
            dma((3, parts)),
            dma((3, parts, 16)),
            dma((3, parts, 2)),
            dma((3, parts, 2)),
            dma((3, parts, 2)),
            dma((3, parts, 2)),
            dma((3, parts, 8)),
            dma((3, 3)),
            dma((3, 4)),
            dma((3, 4)),
            dma((3, 4)),
            dma((parts, 4)),
            dma((parts, 4)),
            dma((parts, 8)),
            dma((parts, 8)),
            dma((2, 2)),
            dma((2, 3)),
            dma((2, 3)),
            dma((2, 2)),
        ],
        compiler_params=pltpu.CompilerParams(
            collective_id=0, has_side_effects=True, vmem_limit_bytes=56 * 2**20
        ),
    )(
        fwd_tokens, back_tokens, out_grad, norm_gain.reshape(1, width),
        gate_weight, up_weight, down_weight, gate_grad_sum,
    )


def body_for(mesh):
    def body(*args):
        tokens, width = args[0].shape
        depth, cols = args[4].shape
        fits = (
            mesh.shape["tp"] == 2 and mesh.shape["fs"] == 16
            and depth == 128 and width == 16 * depth and cols % 128 == 0 and tokens % 128 == 0
        )
        parts = 2 if cols % (8 * 16) == 0 else 1
        if not fits or cols % (4 * parts * 16) != 0:
            return shards(*args)
        return fused_shards(parts, *args)

    return body


def solution(mesh):
    in_specs = (
        P("fs", None),
        P("fs", None),
        P("fs", None),
        P(),
        P("fs", "tp"),
        P("fs", "tp"),
        P("fs", "tp"),
        P("fs", "tp"),
    )
    out_specs = (P("fs", None), P("fs", None), P("fs", "tp"))
    return jax.shard_map(body_for(mesh), mesh=mesh, in_specs=in_specs, out_specs=out_specs, check_vma=False)
```

time: 126 us -> 137 us (1.087)
  Pallas kernels: 119 us -> 131 us
    pallas_call x1, Pallas kernels: 119 us -> 131 us  [fused_shards(): pl.pallas_call(functools.partial(layer_kernel, parts), out_shape=(jax.Sha...]
where the time goes in v1:
time: 137 us; the launch traced here: 135 us
  Pallas kernels  131 us (96%)
  local copies, waits for them, and re-layouts  4.1 us (3%)
    pallas_call x1, Pallas kernels, fused_shards(): pl.pallas_call(functools.partial(layer_kernel, parts), out_shape=(jax.Sha...  131 us
    unnamed x7, local copies, waits for them, and re-layouts  4.1 us

profile of v1, /device:TPU:0, one launch (start us, length us, event | category | flops | bytes accessed | tf_op | source)
XLA Modules:
  0.0 135.5 jit_solution(3685481208207804325)
XLA Ops:
  0.6 130.7 %shard_map.103 = (bf16[128,2048]{1,0:T(8,128)(2,1)}, bf16[128,2048]{1,0:T(8,128)(2,1)}, f32[128,1408]{1,0:T(8,128)}) custom-call(bf16[128,2048]{1,0:T(8,128)(2,1)} %fwd_ref.1, bf16[128,2048]{1,0:T(8,128)(2,1)} %tokens_ref.1, bf16[128,2048]{1,0:T(8,128)(2,1)} %grad_ref.1, f32[1,2048]{1,0:T(1,128)} %bitcast.1, bf16[128,1408]{1,0:T(8,128)(2,1)} %gate_ref.1, ...), custom_call_target="tpu_custom_call" | custom-call | tf_op jit(solution)/shard_map/pallas_call | solution.py:537
  131.4 0.0 copy-start.1
  131.4 1.9 %copy.14 = bf16[128,2048]{1,0:T(8,128)(2,1)} copy(bf16[128,2048]{1,0:T(8,128)(2,1)} %get-tuple-element.6) | data formatting | bytes 1048576
  133.3 0.0 copy-done.1
  133.3 0.0 copy-start
  133.3 0.8 copy.15
  134.1 0.5 copy-done
  134.6 0.9 copy.16
Async XLA Ops:
  131.4 2.0 %copy-start.1 = (bf16[128,2048]{1,0:T(8,128)(2,1)S(1)}, bf16[128,2048]{1,0:T(8,128)(2,1)}, u32[]{:S(2)}) copy-start(bf16[128,2048]{1,0:T(8,128)(2,1)} %get-tuple-element.7) | copy-start | bytes 1572868
  133.3 1.3 copy-start

commit v2 on v1

v2 whole, which is shorter than its diff:
```python
import functools

import jax
import jax.numpy as jnp
from jax import lax
from jax.experimental import pallas as pl
from jax.experimental.pallas import tpu as pltpu
from jax.sharding import PartitionSpec as P

norm_eps = 0.25


def normalize(tokens, norm_gain):
    values = tokens.astype(jnp.float32)
    factor = lax.rsqrt(jnp.mean(values * values, axis=-1, keepdims=True) + norm_eps)
    return (values, factor, (values * factor * norm_gain).astype(jnp.bfloat16))


def shards(
    fwd_tokens, back_tokens, out_grad, norm_gain, gate_weight, up_weight, down_weight, gate_grad_sum
):
    fwd_normed = normalize(fwd_tokens, norm_gain)[2]
    columns = fwd_normed
    gate_pre = jnp.dot(
        columns,
        lax.all_gather(gate_weight, "fs", axis=0, tiled=True),
        preferred_element_type=jnp.float32,
    )
    up_pre = jnp.dot(
        columns,
        lax.all_gather(up_weight, "fs", axis=0, tiled=True),
        preferred_element_type=jnp.float32,
    )
    hidden = (gate_pre * jax.nn.sigmoid(gate_pre) * up_pre).astype(jnp.bfloat16)
    partial_value = jnp.dot(
        hidden,
        lax.all_gather(down_weight, "fs", axis=0, tiled=True).T,
        preferred_element_type=jnp.float32,
    )
    summed = lax.psum(partial_value.astype(jnp.bfloat16), "tp").astype(jnp.float32)
    fwd_out = (0.5 * summed).astype(jnp.bfloat16)
    gate_whole = lax.all_gather(gate_weight, "fs", axis=0, tiled=True)
    up_whole = lax.all_gather(up_weight, "fs", axis=0, tiled=True)
    down_whole = lax.all_gather(down_weight, "fs", axis=0, tiled=True)
    values, factor, back_normed = normalize(back_tokens, norm_gain)
    gate_pre = jnp.dot(back_normed, gate_whole, preferred_element_type=jnp.float32)
    up_pre = jnp.dot(back_normed, up_whole, preferred_element_type=jnp.float32)
    sigmoid_gate = jax.nn.sigmoid(gate_pre)
    back_hidden = 0.5 * jnp.dot(out_grad, down_whole, preferred_element_type=jnp.float32)
    gate_diff = (
        back_hidden * up_pre * sigmoid_gate * (1.0 + gate_pre * (1.0 - sigmoid_gate))
    ).astype(jnp.bfloat16)
    up_diff = (back_hidden * gate_pre * sigmoid_gate).astype(jnp.bfloat16)
    columns = back_normed
    gate_grad_out = gate_grad_sum + lax.psum_scatter(
        jnp.dot(columns.T, gate_diff, preferred_element_type=jnp.float32),
        "fs",
        scatter_dimension=0,
        tiled=True,
    )
    partial_diff = jnp.dot(gate_diff, gate_whole.T, preferred_element_type=jnp.float32)
    partial_diff = partial_diff + jnp.dot(up_diff, up_whole.T, preferred_element_type=jnp.float32)
    normed_diff = lax.psum(partial_diff.astype(jnp.bfloat16), "tp").astype(jnp.float32)
    scaled = normed_diff * norm_gain
    cubed = factor * factor * factor
    back_grad = (
        factor * scaled - values * cubed * jnp.mean(scaled * values, axis=-1, keepdims=True)
    ).astype(jnp.bfloat16)
    back_grad, gate_grad_out = (back_grad, gate_grad_out)
    return (fwd_out, back_grad, gate_grad_out)


MESH = pl.DeviceIdType.MESH


def wide_dot(a, b):
    return lax.dot_general(a, b, (((1,), (1,)), ((), ())), preferred_element_type=jnp.float32)


def padded(size):
    return (size + 127) // 128 * 128


def layer_kernel(
    split, fwd_ref, tokens_ref, grad_ref, gain_ref, gate_ref, up_ref, down_ref, sum_ref,
    fwd_out, back_out, sum_out,
    turned, normed, toks, weights, staged, back_acc, down_acc, fwd_acc, hidden, diffs, diff_cols,
    early, part, crossed, joined, folded, gathered, grad_send, grad_side, grad_total, grad_pass, grad_recv, grad_turn, turn_recv, grad_cols,
    stage_send, stage_recv, weight_recv, far_send, near_send, other_send, pass_send, side_send,
    tok_send, tok_recv, relay_send, relay_recv, gside_send, gside_recv, glev_send, glev_recv,
    gpass_send, gpass_recv, gturn_send, gturn_recv,
    cross_sem, join_send, join_recv, last_sem,
):
    fs, core = lax.axis_index("fs"), lax.axis_index("tp")
    x, y, z = fs % 2, fs // 2 % 2, fs // 4
    odd = z % 2
    inner = jnp.logical_and(z > 0, z < 3)
    near, far, other = z + 1 - 2 * odd, (z + 2) % 4, 3 - z
    sibling = (fs, 1 - core)
    rows = turned.shape[1] // 4
    starts, sizes = (0, split), (split, rows - split)
    pads = tuple(padded(size) for size in sizes)
    depth = gate_ref.shape[0]
    half = fwd_ref.shape[0] // 2
    slab = half * 4
    width = fwd_ref.shape[1]
    band = 4 * depth

    def chip(to_x, to_y, to_z):
        return (to_z * 4 + to_y * 2 + to_x, core)

    beside, across = chip(1 - x, y, z), chip(x, 1 - y, z)
    y_flip = 1 - y

    barrier = pltpu.get_barrier_semaphore()
    for device in (
        sibling, beside, across, chip(x, y, near), chip(x, y, far), chip(x, y, other),
        chip(x, 1 - y, near), chip(x, 1 - y, far), chip(x, 1 - y, other),
    ):
        pl.semaphore_signal(barrier, inc=1, device_id=device, device_id_type=MESH)

    @pl.loop(0, turned.shape[1] // 128)
    def _(t):
        at = pl.ds(pl.multiple_of(t * 128, 128), 128)
        turned[0, at, :] = gate_ref[:, at].T
        turned[1, at, :] = up_ref[:, at].T
        turned[2, at, :] = down_ref[:, at].T

    pl.semaphore_wait(barrier, 9)

    def remote(src, dst, send, recv, device):
        return pltpu.make_async_remote_copy(
            src_ref=src, dst_ref=dst, send_sem=send, recv_sem=recv, device_id=device, device_id_type=MESH
        )

    def own_rows(h, to_y, to_odd):
        return pl.ds(pl.multiple_of((to_y * 2 + to_odd) * rows + starts[h], 16), sizes[h])

    def held_rows(w, h):
        return pl.ds(3 * starts[h] + w * pads[h], sizes[h])

    def both_rows(w, h, count=1):
        return pl.ds(3 * starts[h] + w * pads[h], count * pads[h])

    def own(w, h, to_y, to_odd):
        return turned.at[w, own_rows(h, to_y, to_odd), :]

    def lanes(src):
        return pl.ds(pl.multiple_of(src * depth, depth), depth)

    def level_lanes(s):
        return pl.ds(pl.multiple_of(s * band, band), band)

    def block(w, h, src):
        return weights.at[held_rows(w, h), lanes(src)]

    def send_block(w, h, src, source, sem, device):
        return remote(source, block(w, h, src), sem, weight_recv.at[w, h, src], device)

    def block_in(w, h, src):
        send_block(w, h, src, block(w, h, src), stage_send.at[w, h, 0], sibling).wait_recv()

    def side(w, h, src, source):
        return send_block(w, h, src, source, side_send.at[w, h, src // 2], beside)

    def held(w, h):
        return remote(own(w, h, 1 - y, 1 - odd), staged.at[held_rows(w, h), :], stage_send.at[w, h, 1], stage_recv.at[w, h], across)

    def send_own(h):
        for w in range(3):
            send_block(w, h, fs, own(w, h, 1 - y, odd), stage_send.at[w, h, 0], across).start()
            held(w, h).start()
            send_block(w, h, fs, own(w, h, y, 1 - odd), near_send.at[w, h, 0], chip(x, y, near)).start()
            send_block(w, h, fs, own(w, h, y, odd), far_send.at[w, h, 0], chip(x, y, far)).start()

            @pl.when(inner)
            def _():
                send_block(w, h, fs, own(w, h, y, 1 - odd), other_send.at[w, h, 0], chip(x, y, other)).start()

            side(w, h, fs, own(w, h, y, odd)).start()

    def keep_own(h):
        for w in range(3):
            weights[held_rows(w, h), lanes(fs)] = turned[w, own_rows(h, y, odd), :]

    def clear_pads():
        for h in range(2):
            if pads[h] > sizes[h]:
                for w in range(3):
                    gap = pl.ds(3 * starts[h] + w * pads[h] + sizes[h], pads[h] - sizes[h])
                    weights[gap, :] = jnp.zeros((pads[h] - sizes[h], width), jnp.bfloat16)

    def stage_in(w, h):
        src = z * 4 + (1 - y) * 2 + x
        held(w, h).wait_recv()
        send_block(w, h, src, staged.at[held_rows(w, h), :], near_send.at[w, h, 1], chip(x, y, near)).start()

        @pl.when(inner)
        def _():
            send_block(w, h, src, staged.at[held_rows(w, h), :], other_send.at[w, h, 1], chip(x, y, other)).start()

        block_in(w, h, src)
        send_block(w, h, src, block(w, h, src), far_send.at[w, h, 1], chip(x, y, far)).start()
        side(w, h, src, block(w, h, src)).start()

    def line_in(h, s, line):
        for w in range(3):
            src = s * 4 + line * 2 + x
            block_in(w, h, src)
            if s is near:

                @pl.when(inner)
                def _():
                    send_block(w, h, src, block(w, h, src), pass_send.at[w, h, int(line is not y)], chip(x, y, far)).start()

            side(w, h, src, block(w, h, src)).start()

    def side_in(w, h, s):
        for line in range(2):
            block_in(w, h, s * 4 + line * 2 + 1 - x)

    me = y * 2 + odd
    at_near, at_across, at_both = y * 2 + 1 - odd, (1 - y) * 2 + odd, (1 - y) * 2 + 1 - odd

    def token_rows(a, at):
        return grad_ref.at[at, :] if a == 2 else normed.at[a, at, :]

    def tok_block(a, h, q):
        return toks.at[a, pl.ds(pl.multiple_of(h * slab + q * half, half), half), :]

    def tok_copy(a, n, q, source, device):
        return remote(source, tok_block(a, core, q), tok_send.at[a, n], tok_recv.at[a, q], device)

    def relay(a, q):
        return remote(tok_block(a, core, q), tok_block(a, core, q), relay_send.at[a, q], relay_recv.at[a, q], sibling)

    def send_tokens(a, n):
        mine = token_rows(a, pl.ds(pl.multiple_of(core * half, half), half))
        tok_copy(a, n, me, mine, (chip(x, y, near), across)[n]).start()

    def normal(a):
        @pl.loop(0, tokens_ref.shape[0] // 16)
        def _(r):
            at = pl.ds(pl.multiple_of(r * 16, 16), 16)
            normed[a, at, :] = normalize((tokens_ref, fwd_ref)[a][at, :], gain_ref[...])[2]

    def keep_tokens(a):
        for h in range(2):
            toks[a, pl.ds(pl.multiple_of(h * slab + me * half, half), half), :] = token_rows(a, pl.ds(h * half, half))[...]

    def tok_in(a, q):
        tok_copy(a, 0, q, tok_block(a, core, q), sibling).wait_recv()
        if q is at_near:
            tok_copy(a, 2, q, tok_block(a, core, q), across).start()
        relay(a, q).start()

    def relayed(a):
        for q in (at_near, at_across, at_both):
            remote(tok_block(a, 1 - core, q), tok_block(a, 1 - core, q), relay_send.at[a, q], relay_recv.at[a, q], sibling).wait_recv()

    def project(h, kind, levels, first=True):
        a, w, count, into = ((0, 0, 2, back_acc), (2, 2, 1, down_acc), (1, 0, 2, fwd_acc))[kind]
        wide = count * pads[h]
        at_rows = both_rows(w, h, count)
        for t in range(2):
            at_tokens = pl.ds(t * slab, slab)
            value = None if first else into[h, at_tokens, :wide]
            for s in levels:
                at = level_lanes(s)
                term = wide_dot(toks[a, at_tokens, at], weights[at_rows, at])
                value = term if value is None else value + term
            into[h, at_tokens, :wide] = value

    piece = 64

    def back_parts(h):
        n = pads[h]

        @pl.loop(0, 2 * slab // piece)
        def _(r):
            at = pl.ds(pl.multiple_of(r * piece, piece), piece)
            gate, up = back_acc[h, at, :n], back_acc[h, at, n : 2 * n]
            s = jax.nn.sigmoid(gate)
            back = 0.5 * down_acc[h, at, :n]
            gate_diff = (back * up * s * (1.0 + gate * (1.0 - s))).astype(jnp.bfloat16)
            diff_cols[h, at, :n] = gate_diff
            diffs[h, at, :n] = gate_diff
            diffs[h, at, n : 2 * n] = (back * gate * s).astype(jnp.bfloat16)

    def fwd_parts(h):
        n = pads[h]

        @pl.loop(0, 2 * slab // piece)
        def _(r):
            at = pl.ds(pl.multiple_of(r * piece, piece), piece)
            gate, up = fwd_acc[h, at, :n], fwd_acc[h, at, n : 2 * n]
            hidden[h, at, :n] = (gate * jax.nn.sigmoid(gate) * up).astype(jnp.bfloat16)

    def grad_rows(h):
        return pl.ds(starts[h], sizes[h])

    def grad_across(h, n):
        pair = pl.ds((other, far, near, z)[n] * 2, 2)
        return remote(
            grad_send.at[1 - x, pair, grad_rows(h)], grad_side.at[pair, grad_rows(h)], gside_send.at[h, n], gside_recv.at[h, n], beside
        )

    def grad_make(h):
        diff_turned = diff_cols[h, :, : sizes[h]].T
        for s in range(4):
            at = level_lanes(s)
            product = jnp.dot(diff_turned, toks[0, :, at], preferred_element_type=jnp.float32)
            product = product.astype(jnp.bfloat16)
            for q in range(4):
                grad_send[q % 2, s * 2 + q // 2, grad_rows(h), :] = product[:, q * depth : (q + 1) * depth]

    def grad_out(h):
        for s in range(4):
            grad_across(h, s).start()

    def grad_to(h, n):
        s = (near, far, other)[n]
        source = grad_total.at[pl.ds(s * 2, 2), grad_rows(h)]
        return remote(source, grad_recv.at[n, :, grad_rows(h)], glev_send.at[h, n], glev_recv.at[h, n], chip(x, y, s))

    def grad_past(h):
        source = grad_total.at[pl.ds(other * 2, 2), grad_rows(h)]
        return remote(source, grad_pass.at[:, grad_rows(h)], gpass_send.at[h], gpass_recv.at[h], chip(x, y, far))

    def grad_turned(h):
        return remote(
            grad_turn.at[:, grad_rows(h)], turn_recv.at[:, grad_rows(h)], gturn_send.at[h], gturn_recv.at[h], across
        )

    def grad_on(h, n):
        grad_across(h, n).wait_recv()
        for line in range(2):
            j = (other, far, near, z)[n] * 2 + line
            total = grad_send[x, j, grad_rows(h), :].astype(jnp.float32) + grad_side[j, grad_rows(h), :].astype(jnp.float32)
            grad_total[j, grad_rows(h), :] = total.astype(jnp.bfloat16)
        if n == 0:

            @pl.when(inner)
            def _():
                grad_to(h, 2).start()

            @pl.when(jnp.logical_not(inner))
            def _():
                grad_past(h).start()

        if n == 1:
            grad_to(h, 1).start()
        if n == 2:

            @pl.when(jnp.logical_not(inner))
            def _():
                grad_to(h, 0).start()

    def grad_mid(h):
        @pl.when(inner)
        def _():
            grad_past(h).wait_recv()
            for line in range(2):
                j = near * 2 + line
                total = grad_total[j, grad_rows(h), :].astype(jnp.float32) + grad_pass[line, grad_rows(h), :].astype(jnp.float32)
                grad_total[j, grad_rows(h), :] = total.astype(jnp.bfloat16)
            grad_to(h, 0).start()

    def grad_cols_at(h, to_y, to_odd):
        return pl.ds(pl.multiple_of((to_y * 2 + to_odd) * rows + starts[h], 16), sizes[h])

    def grad_cross(h):
        at = grad_rows(h)
        for n in range(2):
            grad_to(h, n).wait_recv()

        @pl.when(inner)
        def _():
            grad_to(h, 2).wait_recv()
            for line in range(2):
                total = grad_recv[0, line, at, :].astype(jnp.float32) + grad_recv[2, line, at, :].astype(jnp.float32)
                grad_recv[0, line, at, :] = total.astype(jnp.bfloat16)

        def sums(line):
            same = grad_total[z * 2 + line, at, :].astype(jnp.float32) + grad_recv[1, line, at, :].astype(jnp.float32)
            return same, grad_recv[0, line, at, :]

        same, unlike = sums(1 - y)
        grad_turn[0, at, :] = same.astype(jnp.bfloat16)
        grad_turn[1, at, :] = unlike
        grad_turned(h).start()
        same, unlike = sums(y)
        grad_cols[grad_cols_at(h, y, odd), :] = same
        grad_cols[grad_cols_at(h, y, 1 - odd), :] = unlike.astype(jnp.float32)

    def grad_in(h):
        grad_turned(h).wait_recv()
        for n, to_odd in enumerate((odd, 1 - odd)):
            grad_cols[grad_cols_at(h, 1 - y, to_odd), :] = turn_recv[n, grad_rows(h), :].astype(jnp.float32)

    span = width // 2

    def columns(c):
        return pl.ds(c * span, span)

    def cross(k, c):
        at = columns(c)
        return remote(
            part.at[k, 1 - core, :, at], crossed.at[k, :, at], cross_sem.at[k, c, 0], cross_sem.at[k, c, 1], sibling
        )

    strip = 512

    def product_of(k, h, rows_at, at):
        n = pads[h]
        if k == 0:
            return jnp.dot(hidden[h, rows_at, :n], weights[both_rows(2, h), at], preferred_element_type=jnp.float32)
        return jnp.dot(diffs[h, rows_at, : 2 * n], weights[both_rows(0, h, 2), at], preferred_element_type=jnp.float32)

    def partial_early(k):
        @pl.loop(0, width // strip)
        def _(c):
            at = pl.ds(pl.multiple_of(c * strip, strip), strip)
            early[k, :, at] = product_of(k, 0, slice(None), at)

    def partial(k, t, c):
        rows_at = pl.ds(pl.multiple_of(t * slab, slab), slab)
        at = columns(c)
        part[k, t, :, at] = (early[k, rows_at, at] + product_of(k, 1, rows_at, at)).astype(jnp.bfloat16)

    routes = ((across, at_across, at_near, chip(x, y, near)), (chip(x, y, near), at_near, at_across, across))
    routed = ((0, 0), (1, 0))
    def join_copy(k, c, n):
        to, theirs, mine, on = routes[routed[k][c]]
        at = columns(c)
        if n == 2:
            source, device = folded.at[k, :, at], on
        else:
            source, device = joined.at[k, (at_both, theirs)[n], :, at], to
        return remote(source, gathered.at[k, n, :, at], join_send.at[k, c, n], join_recv.at[k, c, n], device)

    def join_start(k, c):
        cross(k, c).wait_recv()
        at = columns(c)
        for n, q in enumerate((at_both, *routes[routed[k][c]][1:3], me)):
            rows_at = pl.ds(pl.multiple_of(q * half, half), half)
            total = part[k, core, rows_at, at].astype(jnp.float32) + crossed[k, rows_at, at].astype(jnp.float32)
            joined[k, q, :, at] = total.astype(jnp.bfloat16)
            if n < 2:
                join_copy(k, c, n).start()

    def join_fold(k, c):
        at = columns(c)
        join_copy(k, c, 0).wait_recv()
        total = gathered[k, 0, :, at].astype(jnp.float32) + joined[k, routes[routed[k][c]][2], :, at].astype(jnp.float32)
        folded[k, :, at] = total.astype(jnp.bfloat16)
        join_copy(k, c, 2).start()

    levels = (z, near, far, other)

    def sides_in(h, some):
        for w in range(3):
            for s in some:
                side_in(w, h, s)

    def stages_in(h):
        for w in range(3):
            stage_in(w, h)

    send_own(0)
    send_own(1)
    send_tokens(2, 1)
    normal(0)
    send_tokens(0, 1)
    normal(1)
    send_tokens(1, 1)
    clear_pads()
    for h in range(2):
        keep_own(h)
    for a in range(3):
        keep_tokens(a)
    stages_in(0)
    send_tokens(2, 0)
    send_tokens(0, 0)
    send_tokens(1, 0)
    stages_in(1)
    for h in range(2):
        line_in(h, near, y)
        line_in(h, far, y)
    tok_in(2, at_across)
    line_in(0, near, y_flip)
    line_in(0, far, y_flip)
    tok_in(2, at_near)
    tok_in(0, at_across)
    line_in(0, other, y)
    line_in(1, far, y_flip)
    tok_in(0, at_near)
    line_in(1, other, y)
    tok_in(1, at_across)
    tok_in(2, at_both)
    line_in(0, other, y_flip)
    line_in(1, near, y_flip)
    tok_in(0, at_both)
    relayed(2)
    sides_in(0, levels)
    tok_in(1, at_near)
    project(0, 1, levels)
    relayed(0)
    line_in(1, other, y_flip)
    project(0, 0, levels)
    back_parts(0)
    grad_make(0)
    grad_out(0)
    partial_early(1)
    sides_in(1, levels[:3])
    for kind in range(2):
        project(1, kind, levels[:3])
    tok_in(1, at_both)
    relayed(1)
    project(0, 2, levels)
    fwd_parts(0)
    partial_early(0)
    project(1, 2, levels[:3])
    sides_in(1, levels[3:])
    project(1, 0, levels[3:], False)
    project(1, 1, levels[3:], False)
    back_parts(1)
    for c in range(2):
        partial(1, 1 - core, c)
        cross(1, c).start()
    for c in range(2):
        partial(1, core, c)
        join_start(1, c)
    project(1, 2, levels[3:], False)
    fwd_parts(1)
    for c in range(2):
        partial(0, 1 - core, c)
        cross(0, c).start()
    for c in range(2):
        partial(0, core, c)
        join_start(0, c)
    grad_make(1)
    grad_out(1)
    for n in range(4):
        grad_on(0, n)
    for c in range(2):
        join_fold(1, c)
    grad_mid(0)
    for n in range(4):
        grad_on(1, n)
    for c in range(2):
        join_fold(0, c)
    grad_mid(1)
    grad_cross(0)
    grad_cross(1)

    mine = pl.ds(pl.multiple_of(core * half, half), half)

    def last(k):
        out = (fwd_out, back_out)[k]
        return remote(out.at[mine, :], out.at[mine, :], last_sem.at[k, 0], last_sem.at[k, 1], sibling)

    def joined_in(k):
        for c in range(2):
            for n in (1, 2):
                join_copy(k, c, n).wait_recv()

    def total_of(k, at):
        value = joined[k, me, at, :].astype(jnp.float32) + gathered[k, 1, at, :].astype(jnp.float32)
        return value + gathered[k, 2, at, :].astype(jnp.float32)

    small = 16
    joined_in(0)
    for r in range(half // small):
        at = pl.ds(r * small, small)
        fwd_out[pl.ds(pl.multiple_of(core * half + r * small, small), small), :] = (0.5 * total_of(0, at)).astype(jnp.bfloat16)
    last(0).start()
    joined_in(1)
    for r in range(half // small):
        at = pl.ds(r * small, small)
        there = pl.ds(pl.multiple_of(core * half + r * small, small), small)
        values = tokens_ref[there, :].astype(jnp.float32)
        factor = lax.rsqrt(jnp.mean(values * values, axis=-1, keepdims=True) + norm_eps)
        scaled = total_of(1, at) * gain_ref[...]
        cubed = factor * factor * factor
        back_out[there, :] = (
            factor * scaled - values * cubed * jnp.mean(scaled * values, axis=-1, keepdims=True)
        ).astype(jnp.bfloat16)
    last(1).start()

    for h in range(2):
        grad_in(h)

    @pl.loop(0, grad_cols.shape[0] // 128)
    def _(t):
        at = pl.ds(pl.multiple_of(t * 128, 128), 128)
        sum_out[:, at] = sum_ref[:, at] + grad_cols[at, :].T

    for h in range(2):
        for w in range(3):
            for n in range(2):
                gone = block(w, h, fs)
                for sem in (stage_send, near_send, far_send):
                    send_block(w, h, fs, gone, sem.at[w, h, n], sibling).wait_send()

                @pl.when(inner)
                def _():
                    for sem in (other_send, pass_send):
                        send_block(w, h, fs, gone, sem.at[w, h, n], sibling).wait_send()

            @pl.loop(0, 8)
            def _(j):
                send_block(w, h, fs, gone, side_send.at[w, h, j], sibling).wait_send()

        for s in range(4):
            grad_across(h, s).wait_send()
        grad_to(h, 0).wait_send()
        grad_to(h, 1).wait_send()
        grad_turned(h).wait_send()

        @pl.when(inner)
        def _():
            grad_to(h, 2).wait_send()

        @pl.when(jnp.logical_not(inner))
        def _():
            grad_past(h).wait_send()

    for a in range(3):
        for n in range(3):
            tok_copy(a, n, me, tok_block(a, core, me), sibling).wait_send()
        for q in (at_near, at_across, at_both):
            relay(a, q).wait_send()
    for k in range(2):
        for c in range(2):
            cross(k, c).wait_send()
            for n in range(3):
                join_copy(k, c, n).wait_send()
        last(k).wait()


def fused_shards(
    split, fwd_tokens, back_tokens, out_grad, norm_gain, gate_weight, up_weight, down_weight, gate_grad_sum
):
    tokens, width = fwd_tokens.shape
    depth, cols = gate_weight.shape
    rows = cols // 4
    wide = max(padded(split), padded(rows - split))
    held = 3 * (padded(split) + padded(rows - split))
    half = tokens // 2
    slab = half * 4
    narrow, full = jnp.bfloat16, jnp.float32
    dma = pltpu.SemaphoreType.DMA
    vmem = pl.BlockSpec(memory_space=pltpu.VMEM)
    return pl.pallas_call(
        functools.partial(layer_kernel, split),
        out_shape=(
            jax.ShapeDtypeStruct((tokens, width), narrow),
            jax.ShapeDtypeStruct((tokens, width), narrow),
            jax.ShapeDtypeStruct((depth, cols), full),
        ),
        in_specs=[vmem] * 8,
        out_specs=(vmem,) * 3,
        scratch_shapes=[
            pltpu.VMEM((3, cols, depth), narrow),
            pltpu.VMEM((2, tokens, width), narrow),
            pltpu.VMEM((3, 2 * slab, width), narrow),
            pltpu.VMEM((held, width), narrow),
            pltpu.VMEM((held, depth), narrow),
            pltpu.VMEM((2, 2 * slab, 2 * wide), full),
            pltpu.VMEM((2, 2 * slab, wide), full),
            pltpu.VMEM((2, 2 * slab, 2 * wide), full),
            pltpu.VMEM((2, 2 * slab, wide), narrow),
            pltpu.VMEM((2, 2 * slab, 2 * wide), narrow),
            pltpu.VMEM((2, 2 * slab, wide), narrow),
            pltpu.VMEM((2, 2 * slab, width), full),
            pltpu.VMEM((2, 2, slab, width), narrow),
            pltpu.VMEM((2, slab, width), narrow),
            pltpu.VMEM((2, 4, half, width), narrow),
            pltpu.VMEM((2, half, width), narrow),
            pltpu.VMEM((2, 3, half, width), narrow),
            pltpu.VMEM((2, 8, rows, depth), narrow),
            pltpu.VMEM((8, rows, depth), narrow),
            pltpu.VMEM((8, rows, depth), narrow),
            pltpu.VMEM((2, rows, depth), narrow),
            pltpu.VMEM((3, 2, rows, depth), narrow),
            pltpu.VMEM((2, rows, depth), narrow),
            pltpu.VMEM((2, rows, depth), narrow),
            pltpu.VMEM((cols, depth), full),
            dma((3, 2, 2)),
            dma((3, 2)),
            dma((3, 2, 16)),
            dma((3, 2, 2)),
            dma((3, 2, 2)),
            dma((3, 2, 2)),
            dma((3, 2, 2)),
            dma((3, 2, 8)),
            dma((3, 3)),
            dma((3, 4)),
            dma((3, 4)),
            dma((3, 4)),
            dma((2, 4)),
            dma((2, 4)),
            dma((2, 3)),
            dma((2, 3)),
            dma((2,)),
            dma((2,)),
            dma((2,)),
            dma((2,)),
            dma((2, 2, 2)),
            dma((2, 2, 3)),
            dma((2, 2, 3)),
            dma((2, 2)),
        ],
        compiler_params=pltpu.CompilerParams(
            collective_id=0, has_side_effects=True, vmem_limit_bytes=60 * 2**20
        ),
    )(
        fwd_tokens, back_tokens, out_grad, norm_gain.reshape(1, width),
        gate_weight, up_weight, down_weight, gate_grad_sum,
    )


def body_for(mesh):
    def body(*args):
        tokens, width = args[0].shape
        depth, cols = args[4].shape
        rows = cols // 4
        fits = (
            mesh.shape["tp"] == 2 and mesh.shape["fs"] == 16
            and depth == 128 and width == 16 * depth and cols % 128 == 0 and tokens % 128 == 0
            and rows > 256 and rows % 16 == 0
        )
        if not fits:
            return shards(*args)
        return fused_shards((rows - 1) // 256 * 256, *args)

    return body


def solution(mesh):
    in_specs = (
        P("fs", None),
        P("fs", None),
        P("fs", None),
        P(),
        P("fs", "tp"),
        P("fs", "tp"),
        P("fs", "tp"),
        P("fs", "tp"),
    )
    out_specs = (P("fs", None), P("fs", None), P("fs", "tp"))
    return jax.shard_map(body_for(mesh), mesh=mesh, in_specs=in_specs, out_specs=out_specs, check_vma=False)
```

time: 137 us -> 112 us (0.82)
  Pallas kernels: 131 us -> 107 us
    pallas_call x1, Pallas kernels: 131 us -> 107 us  [fused_shards(): pl.pallas_call(functools.partial(layer_kernel, split), out_shape=(jax.Sha...]
where the time goes in v2:
time: 112 us
  Pallas kernels  107 us (96%)
  local copies, waits for them, and re-layouts  4.1 us (4%)
    pallas_call x1, Pallas kernels, fused_shards(): pl.pallas_call(functools.partial(layer_kernel, split), out_shape=(jax.Sha...  107 us
    unnamed x7, local copies, waits for them, and re-layouts  4.1 us

profile of v2, /device:TPU:0, one launch (start us, length us, event | category | flops | bytes accessed | tf_op | source)
XLA Modules:
  0.0 111.7 jit_solution(7918225020442348400)
XLA Ops:
  0.6 106.9 %shard_map.103 = (bf16[128,2048]{1,0:T(8,128)(2,1)}, bf16[128,2048]{1,0:T(8,128)(2,1)}, f32[128,1408]{1,0:T(8,128)}) custom-call(bf16[128,2048]{1,0:T(8,128)(2,1)} %fwd_ref.1, bf16[128,2048]{1,0:T(8,128)(2,1)} %tokens_ref.1, bf16[128,2048]{1,0:T(8,128)(2,1)} %grad_ref.1, f32[1,2048]{1,0:T(1,128)} %bitcast.1, bf16[128,1408]{1,0:T(8,128)(2,1)} %gate_ref.1, ...), custom_call_target="tpu_custom_call" | custom-call | tf_op jit(solution)/shard_map/pallas_call | solution.py:655
  107.6 0.0 copy-start.1
  107.6 1.9 %copy.14 = bf16[128,2048]{1,0:T(8,128)(2,1)} copy(bf16[128,2048]{1,0:T(8,128)(2,1)} %get-tuple-element.6) | data formatting | bytes 1048576
  109.5 0.0 copy-done.1
  109.5 0.0 copy-start
  109.5 0.8 copy.15
  110.3 0.5 copy-done
  110.8 0.9 copy.16
Async XLA Ops:
  107.6 2.0 %copy-start.1 = (bf16[128,2048]{1,0:T(8,128)(2,1)S(1)}, bf16[128,2048]{1,0:T(8,128)(2,1)}, u32[]{:S(2)}) copy-start(bf16[128,2048]{1,0:T(8,128)(2,1)} %get-tuple-element.7) | copy-start | bytes 1572868
  109.5 1.3 %copy-start = (f32[128,1408]{1,0:T(8,128)S(1)}, f32[128,1408]{1,0:T(8,128)}, u32[]{:S(2)}) copy-start(f32[128,1408]{1,0:T(8,128)} %get-tuple-element.8) | copy-start | bytes 2162692

commit v3 on v2

--- a/solution.py
+++ b/solution.py
@@ -8,6 +8,7 @@
 from jax.sharding import PartitionSpec as P
 
 norm_eps = 0.25
+vmem_bytes = 66_900_000
 
 
 def normalize(tokens, norm_gain):
@@ -82,14 +83,14 @@
 
 
 def layer_kernel(
-    split, fwd_ref, tokens_ref, grad_ref, gain_ref, gate_ref, up_ref, down_ref, sum_ref,
+    split, fwd_in, tokens_in, grad_in_ref, gain_ref, gate_in, up_in, down_in, sum_in,
     fwd_out, back_out, sum_out,
-    turned, normed, toks, weights, staged, back_acc, down_acc, fwd_acc, hidden, diffs, diff_cols,
-    early, part, crossed, joined, folded, gathered, grad_send, grad_side, grad_total, grad_pass, grad_recv, grad_turn, turn_recv, grad_cols,
+    raw, raw_tokens, sum_ref, turned, normed, toks, weights, staged, back_acc, down_acc, fwd_acc, hidden, diffs, diff_cols,
+    part, crossed, joined, folded, gathered, grad_send, grad_side, grad_total, grad_pass, grad_recv, grad_turn, turn_recv, grad_cols,
     stage_send, stage_recv, weight_recv, far_send, near_send, other_send, pass_send, side_send,
     tok_send, tok_recv, relay_send, relay_recv, gside_send, gside_recv, glev_send, glev_recv,
     gpass_send, gpass_recv, gturn_send, gturn_recv,
-    cross_sem, join_send, join_recv, last_sem,
+    cross_sem, join_send, join_recv, last_sem, raw_sem, token_sem, sum_sem,
 ):
     fs, core = lax.axis_index("fs"), lax.axis_index("tp")
     x, y, z = fs % 2, fs // 2 % 2, fs // 4
@@ -100,10 +101,11 @@
     rows = turned.shape[1] // 4
     starts, sizes = (0, split), (split, rows - split)
     pads = tuple(padded(size) for size in sizes)
-    depth = gate_ref.shape[0]
-    half = fwd_ref.shape[0] // 2
+    depth = gate_in.shape[0]
+    half = fwd_in.shape[0] // 2
+    tokens_ref, fwd_ref, grad_ref = raw_tokens.at[0], raw_tokens.at[1], raw_tokens.at[2]
     slab = half * 4
-    width = fwd_ref.shape[1]
+    width = fwd_in.shape[1]
     band = 4 * depth
 
     def chip(to_x, to_y, to_z):
@@ -119,14 +121,19 @@
     ):
         pl.semaphore_signal(barrier, inc=1, device_id=device, device_id_type=MESH)
 
-    @pl.loop(0, turned.shape[1] // 128)
-    def _(t):
-        at = pl.ds(pl.multiple_of(t * 128, 128), 128)
-        turned[0, at, :] = gate_ref[:, at].T
-        turned[1, at, :] = up_ref[:, at].T
-        turned[2, at, :] = down_ref[:, at].T
-
-    pl.semaphore_wait(barrier, 9)
+    raw_copies = [pltpu.make_async_copy(ref, raw.at[w], raw_sem.at[w]) for w, ref in enumerate((gate_in, up_in, down_in))]
+    token_copies = [
+        pltpu.make_async_copy(ref, raw_tokens.at[a], token_sem.at[a]) for a, ref in enumerate((tokens_in, fwd_in, grad_in_ref))
+    ]
+    sum_copy = pltpu.make_async_copy(sum_in, sum_ref, sum_sem.at[0])
+    for copy in (*raw_copies, token_copies[2], token_copies[0], token_copies[1], sum_copy):
+        copy.start()
+
+    def turn_in(w):
+        raw_copies[w].wait()
+        for n in range(turned.shape[1] // 128):
+            at = pl.ds(n * 128, 128)
+            turned[w, at, :] = raw[w, :, at].T
 
     def remote(src, dst, send, recv, device):
         return pltpu.make_async_remote_copy(
@@ -166,10 +173,13 @@
     def held(w, h):
         return remote(own(w, h, 1 - y, 1 - odd), staged.at[held_rows(w, h), :], stage_send.at[w, h, 1], stage_recv.at[w, h], across)
 
-    def send_own(h):
-        for w in range(3):
+    def send_stage(h, some=range(3)):
+        for w in some:
             send_block(w, h, fs, own(w, h, 1 - y, odd), stage_send.at[w, h, 0], across).start()
             held(w, h).start()
+
+    def send_own(h, some=range(3)):
+        for w in some:
             send_block(w, h, fs, own(w, h, y, 1 - odd), near_send.at[w, h, 0], chip(x, y, near)).start()
             send_block(w, h, fs, own(w, h, y, odd), far_send.at[w, h, 0], chip(x, y, far)).start()
 
@@ -215,9 +225,10 @@
 
             side(w, h, src, block(w, h, src)).start()
 
-    def side_in(w, h, s):
-        for line in range(2):
-            block_in(w, h, s * 4 + line * 2 + 1 - x)
+    def sides_in(h, groups):
+        for w in range(3):
+            for s, line in groups:
+                block_in(w, h, s * 4 + line * 2 + 1 - x)
 
     me = y * 2 + odd
     at_near, at_across, at_both = y * 2 + 1 - odd, (1 - y) * 2 + odd, (1 - y) * 2 + 1 - odd
@@ -258,15 +269,15 @@
         for q in (at_near, at_across, at_both):
             remote(tok_block(a, 1 - core, q), tok_block(a, 1 - core, q), relay_send.at[a, q], relay_recv.at[a, q], sibling).wait_recv()
 
-    def project(h, kind, levels, first=True):
+    def project(h, kind, groups, first=False):
         a, w, count, into = ((0, 0, 2, back_acc), (2, 2, 1, down_acc), (1, 0, 2, fwd_acc))[kind]
         wide = count * pads[h]
         at_rows = both_rows(w, h, count)
         for t in range(2):
             at_tokens = pl.ds(t * slab, slab)
             value = None if first else into[h, at_tokens, :wide]
-            for s in levels:
-                at = level_lanes(s)
+            for s, line in groups:
+                at = pl.ds(pl.multiple_of((s * 4 + line * 2) * depth, 2 * depth), 2 * depth)
                 term = wide_dot(toks[a, at_tokens, at], weights[at_rows, at])
                 value = term if value is None else value + term
             into[h, at_tokens, :wide] = value
@@ -417,16 +428,10 @@
             return jnp.dot(hidden[h, rows_at, :n], weights[both_rows(2, h), at], preferred_element_type=jnp.float32)
         return jnp.dot(diffs[h, rows_at, : 2 * n], weights[both_rows(0, h, 2), at], preferred_element_type=jnp.float32)
 
-    def partial_early(k):
-        @pl.loop(0, width // strip)
-        def _(c):
-            at = pl.ds(pl.multiple_of(c * strip, strip), strip)
-            early[k, :, at] = product_of(k, 0, slice(None), at)
-
     def partial(k, t, c):
         rows_at = pl.ds(pl.multiple_of(t * slab, slab), slab)
         at = columns(c)
-        part[k, t, :, at] = (early[k, rows_at, at] + product_of(k, 1, rows_at, at)).astype(jnp.bfloat16)
+        part[k, t, :, at] = (product_of(k, 0, rows_at, at) + product_of(k, 1, rows_at, at)).astype(jnp.bfloat16)
 
     routes = ((across, at_across, at_near, chip(x, y, near)), (chip(x, y, near), at_near, at_across, across))
     routed = ((0, 0), (1, 0))
@@ -456,109 +461,128 @@
         folded[k, :, at] = total.astype(jnp.bfloat16)
         join_copy(k, c, 2).start()
 
-    levels = (z, near, far, other)
-
-    def sides_in(h, some):
-        for w in range(3):
-            for s in some:
-                side_in(w, h, s)
-
     def stages_in(h):
         for w in range(3):
             stage_in(w, h)
 
-    send_own(0)
-    send_own(1)
+    first_far = (jnp.where(inner, other, far), jnp.where(inner, y, y_flip))
+    next_far = (other, jnp.where(inner, y_flip, y))
+    last_far = (jnp.where(inner, far, other), y_flip)
+    home = ((z, y), (z, y_flip))
+    soon = ((near, y), (far, y), first_far)
+    late = ((near, y_flip), next_far, last_far)
+
+    def down_parts(k):
+        for c in range(2):
+            partial(k, 1 - core, c)
+            cross(k, c).start()
+        for c in range(2):
+            partial(k, core, c)
+
+    for w in range(3):
+        turn_in(w)
+        if w == 0:
+            pl.semaphore_wait(barrier, 9)
+        send_stage(0, (w,))
+        send_own(0, (w,))
+    token_copies[2].wait()
     send_tokens(2, 1)
+    send_tokens(2, 0)
+    token_copies[0].wait()
     normal(0)
     send_tokens(0, 1)
+    send_tokens(0, 0)
+    send_own(1)
+    token_copies[1].wait()
     normal(1)
-    send_tokens(1, 1)
     clear_pads()
     for h in range(2):
         keep_own(h)
     for a in range(3):
         keep_tokens(a)
     stages_in(0)
-    send_tokens(2, 0)
-    send_tokens(0, 0)
     send_tokens(1, 0)
+    line_in(0, near, y)
+    line_in(0, far, y)
+    tok_in(2, at_across)
+    tok_in(2, at_near)
+    send_stage(1)
+    line_in(0, *first_far)
+    tok_in(0, at_across)
+    line_in(1, far, y)
+    tok_in(0, at_near)
+    send_tokens(1, 1)
+    line_in(0, *next_far)
+    line_in(1, near, y)
     stages_in(1)
-    for h in range(2):
-        line_in(h, near, y)
-        line_in(h, far, y)
-    tok_in(2, at_across)
+    tok_in(2, at_both)
     line_in(0, near, y_flip)
-    line_in(0, far, y_flip)
-    tok_in(2, at_near)
-    tok_in(0, at_across)
-    line_in(0, other, y)
-    line_in(1, far, y_flip)
-    tok_in(0, at_near)
-    line_in(1, other, y)
+    relayed(2)
+    line_in(1, *first_far)
+    sides_in(0, home)
+    project(0, 1, home, True)
+    tok_in(0, at_both)
+    line_in(1, *next_far)
+    relayed(0)
+    project(0, 0, home, True)
     tok_in(1, at_across)
-    tok_in(2, at_both)
-    line_in(0, other, y_flip)
+    sides_in(0, soon)
+    project(0, 1, soon)
+    line_in(0, *last_far)
+    project(0, 0, soon)
+    tok_in(1, at_near)
+    sides_in(1, home)
+    project(1, 0, home, True)
+    project(1, 1, home, True)
     line_in(1, near, y_flip)
-    tok_in(0, at_both)
-    relayed(2)
-    sides_in(0, levels)
-    tok_in(1, at_near)
-    project(0, 1, levels)
-    relayed(0)
-    line_in(1, other, y_flip)
-    project(0, 0, levels)
+    line_in(1, *last_far)
+    sides_in(1, soon)
+    project(1, 0, soon)
+    project(1, 1, soon)
+    sides_in(0, late)
+    project(0, 1, late)
+    project(0, 0, late)
     back_parts(0)
     grad_make(0)
     grad_out(0)
-    partial_early(1)
-    sides_in(1, levels[:3])
-    for kind in range(2):
-        project(1, kind, levels[:3])
     tok_in(1, at_both)
-    relayed(1)
-    project(0, 2, levels)
-    fwd_parts(0)
-    partial_early(0)
-    project(1, 2, levels[:3])
-    sides_in(1, levels[3:])
-    project(1, 0, levels[3:], False)
-    project(1, 1, levels[3:], False)
+    sides_in(1, late)
+    project(1, 0, late)
+    project(1, 1, late)
     back_parts(1)
-    for c in range(2):
-        partial(1, 1 - core, c)
-        cross(1, c).start()
-    for c in range(2):
-        partial(1, core, c)
-        join_start(1, c)
-    project(1, 2, levels[3:], False)
-    fwd_parts(1)
-    for c in range(2):
-        partial(0, 1 - core, c)
-        cross(0, c).start()
-    for c in range(2):
-        partial(0, core, c)
-        join_start(0, c)
+    down_parts(1)
     grad_make(1)
     grad_out(1)
-    for n in range(4):
-        grad_on(0, n)
+    for c in range(2):
+        join_start(1, c)
+    relayed(1)
+    project(0, 2, home + soon + late, True)
+    fwd_parts(0)
+    grad_on(0, 0)
+    project(1, 2, home + soon + late, True)
+    fwd_parts(1)
+    down_parts(0)
+    grad_on(0, 1)
+    for c in range(2):
+        join_start(0, c)
+    grad_on(0, 2)
+    grad_on(0, 3)
+    grad_mid(0)
     for c in range(2):
         join_fold(1, c)
-    grad_mid(0)
     for n in range(4):
         grad_on(1, n)
+    grad_mid(1)
     for c in range(2):
         join_fold(0, c)
-    grad_mid(1)
     grad_cross(0)
     grad_cross(1)
 
     mine = pl.ds(pl.multiple_of(core * half, half), half)
 
     def last(k):
-        out = (fwd_out, back_out)[k]
-        return remote(out.at[mine, :], out.at[mine, :], last_sem.at[k, 0], last_sem.at[k, 1], sibling)
+        out = (fwd_out, back_out)[k].at[mine, :]
+        return remote(out, out, last_sem.at[k, 0], last_sem.at[k, 1], sibling)
 
     def joined_in(k):
         for c in range(2):
@@ -569,32 +593,40 @@
         value = joined[k, me, at, :].astype(jnp.float32) + gathered[k, 1, at, :].astype(jnp.float32)
         return value + gathered[k, 2, at, :].astype(jnp.float32)
 
+    tiles = grad_cols.shape[0] // 128
+    early = rows * 2 // 128
+
+    def grad_tiles(first, count):
+        @pl.loop(0, count)
+        def _(n):
+            at = pl.ds(pl.multiple_of((first + n) * 128, 128), 128)
+            sum_out[:, at] = sum_ref[:, at] + grad_cols[at, :].T
+
     small = 16
+
+    def out_rows(r):
+        return pl.ds(pl.multiple_of(core * half + r * small, small), small)
+
+    sum_copy.wait()
+    grad_tiles(y * (tiles - early), early)
     joined_in(0)
     for r in range(half // small):
-        at = pl.ds(r * small, small)
-        fwd_out[pl.ds(pl.multiple_of(core * half + r * small, small), small), :] = (0.5 * total_of(0, at)).astype(jnp.bfloat16)
+        fwd_out[out_rows(r), :] = (0.5 * total_of(0, pl.ds(r * small, small))).astype(jnp.bfloat16)
     last(0).start()
     joined_in(1)
     for r in range(half // small):
-        at = pl.ds(r * small, small)
-        there = pl.ds(pl.multiple_of(core * half + r * small, small), small)
-        values = tokens_ref[there, :].astype(jnp.float32)
+        values = tokens_ref[out_rows(r), :].astype(jnp.float32)
         factor = lax.rsqrt(jnp.mean(values * values, axis=-1, keepdims=True) + norm_eps)
-        scaled = total_of(1, at) * gain_ref[...]
+        scaled = total_of(1, pl.ds(r * small, small)) * gain_ref[...]
         cubed = factor * factor * factor
-        back_out[there, :] = (
+        back_out[out_rows(r), :] = (
             factor * scaled - values * cubed * jnp.mean(scaled * values, axis=-1, keepdims=True)
         ).astype(jnp.bfloat16)
     last(1).start()
 
     for h in range(2):
         grad_in(h)
-
-    @pl.loop(0, grad_cols.shape[0] // 128)
-    def _(t):
-        at = pl.ds(pl.multiple_of(t * 128, 128), 128)
-        sum_out[:, at] = sum_ref[:, at] + grad_cols[at, :].T
+    grad_tiles((1 - y) * early, tiles - early)
 
     for h in range(2):
         for w in range(3):
@@ -645,6 +677,7 @@
     tokens, width = fwd_tokens.shape
     depth, cols = gate_weight.shape
     rows = cols // 4
+    out_bytes = 2 * tokens * width * 2 + depth * cols * 4
     wide = max(padded(split), padded(rows - split))
     held = 3 * (padded(split) + padded(rows - split))
     half = tokens // 2
@@ -652,16 +685,20 @@
     narrow, full = jnp.bfloat16, jnp.float32
     dma = pltpu.SemaphoreType.DMA
     vmem = pl.BlockSpec(memory_space=pltpu.VMEM)
+    hbm = pl.BlockSpec(memory_space=pl.ANY)
     return pl.pallas_call(
         functools.partial(layer_kernel, split),
         out_shape=(
-            jax.ShapeDtypeStruct((tokens, width), narrow),
-            jax.ShapeDtypeStruct((tokens, width), narrow),
-            jax.ShapeDtypeStruct((depth, cols), full),
+            pltpu.VMEM((tokens, width), narrow),
+            pltpu.VMEM((tokens, width), narrow),
+            pltpu.VMEM((depth, cols), full),
         ),
-        in_specs=[vmem] * 8,
+        in_specs=[hbm] * 3 + [vmem] + [hbm] * 4,
         out_specs=(vmem,) * 3,
         scratch_shapes=[
+            pltpu.VMEM((3, depth, cols), narrow),
+            pltpu.VMEM((3, tokens, width), narrow),
+            pltpu.VMEM((depth, cols), full),
             pltpu.VMEM((3, cols, depth), narrow),
             pltpu.VMEM((2, tokens, width), narrow),
             pltpu.VMEM((3, 2 * slab, width), narrow),
@@ -673,7 +710,6 @@
             pltpu.VMEM((2, 2 * slab, wide), narrow),
             pltpu.VMEM((2, 2 * slab, 2 * wide), narrow),
             pltpu.VMEM((2, 2 * slab, wide), narrow),
-            pltpu.VMEM((2, 2 * slab, width), full),
             pltpu.VMEM((2, 2, slab, width), narrow),
             pltpu.VMEM((2, slab, width), narrow),
             pltpu.VMEM((2, 4, half, width), narrow),
@@ -711,9 +747,12 @@
             dma((2, 2, 3)),
             dma((2, 2, 3)),
             dma((2, 2)),
+            dma((3,)),
+            dma((3,)),
+            dma((1,)),
         ],
         compiler_params=pltpu.CompilerParams(
-            collective_id=0, has_side_effects=True, vmem_limit_bytes=60 * 2**20
+            collective_id=0, has_side_effects=True, vmem_limit_bytes=vmem_bytes - out_bytes
         ),
     )(
         fwd_tokens, back_tokens, out_grad, norm_gain.reshape(1, width),

time: 112 us -> 104 us (0.929)
  Pallas kernels: 107 us -> 101 us
  local copies, waits for them, and re-layouts: 4.1 us -> 2.45 us
    pallas_call x1, Pallas kernels: 107 us -> 101 us  [fused_shards(): pl.pallas_call(functools.partial(layer_kernel, split), out_shape=(pltpu.V...]
    unnamed x7 -> x3, local copies, waits for them, and re-layouts: 4.1 us -> 2.45 us
where the time goes in v3:
time: 104 us
  Pallas kernels  101 us (97%)
  local copies, waits for them, and re-layouts  2.45 us (2%)
    pallas_call x1, Pallas kernels, fused_shards(): pl.pallas_call(functools.partial(layer_kernel, split), out_shape=(pltpu.V...  101 us
    unnamed x3, local copies, waits for them, and re-layouts  2.45 us

profile of v3, /device:TPU:0, one launch (start us, length us, event | category | flops | bytes accessed | tf_op | source)
XLA Modules:
  0.0 103.9 jit_solution(8114717825666714458)
XLA Ops:
  0.6 100.8 %shard_map.103 = (bf16[128,2048]{1,0:T(8,128)(2,1)S(1)}, bf16[128,2048]{1,0:T(8,128)(2,1)S(1)}, f32[128,1408]{1,0:T(8,128)S(1)}) custom-call(bf16[128,2048]{1,0:T(8,128)(2,1)} %fwd_in.1, bf16[128,2048]{1,0:T(8,128)(2,1)} %tokens_in.1, bf16[128,2048]{1,0:T(8,128)(2,1)} %grad_in_ref.1, f32[1,2048]{1,0:T(1,128)} %bitcast.1, bf16[128,1408]{1,0:T(8,128)(2,1)} %gate_in.1, ...), custom_call_target="tpu_custom_call" | custom-call | tf_op jit(solution)/shard_map/pallas_call | solution.py:689
  101.4 0.8 copy.14
  102.2 0.8 copy.15
  103.0 0.9 copy.16

commit v4 on v3

--- a/solution.py
+++ b/solution.py
@@ -87,10 +87,9 @@
     fwd_out, back_out, sum_out,
     raw, raw_tokens, sum_ref, turned, normed, toks, weights, staged, back_acc, down_acc, fwd_acc, hidden, diffs, diff_cols,
     part, crossed, joined, folded, gathered, grad_send, grad_side, grad_total, grad_pass, grad_recv, grad_turn, turn_recv, grad_cols,
-    stage_send, stage_recv, weight_recv, far_send, near_send, other_send, pass_send, side_send,
-    tok_send, tok_recv, relay_send, relay_recv, gside_send, gside_recv, glev_send, glev_recv,
-    gpass_send, gpass_recv, gturn_send, gturn_recv,
-    cross_sem, join_send, join_recv, last_sem, raw_sem, token_sem, sum_sem,
+    block_send, inner_send, line_recv, held_recv, side_recv, tok_send, tok_recv, relay_recv,
+    gside_send, gside_recv, gsend, glev_recv, gpass_recv, gturn_recv,
+    cross_send, cross_recv, join_send, fold_recv, join_recv, last_send, last_recv, raw_sem, token_sem, sum_sem,
 ):
     fs, core = lax.axis_index("fs"), lax.axis_index("tp")
     x, y, z = fs % 2, fs // 2 % 2, fs // 4
@@ -140,6 +139,12 @@
             src_ref=src, dst_ref=dst, send_sem=send, recv_sem=recv, device_id=device, device_id_type=MESH
         )
 
+    def got(ref, sem):
+        remote(ref, ref, sem, sem, sibling).wait_recv()
+
+    def gone(ref, sem):
+        remote(ref, ref, sem, sem, sibling).wait_send()
+
     def own_rows(h, to_y, to_odd):
         return pl.ds(pl.multiple_of((to_y * 2 + to_odd) * rows + starts[h], 16), sizes[h])
 
@@ -161,33 +166,58 @@
     def block(w, h, src):
         return weights.at[held_rows(w, h), lanes(src)]
 
-    def send_block(w, h, src, source, sem, device):
-        return remote(source, block(w, h, src), sem, weight_recv.at[w, h, src], device)
-
-    def block_in(w, h, src):
-        send_block(w, h, src, block(w, h, src), stage_send.at[w, h, 0], sibling).wait_recv()
-
-    def side(w, h, src, source):
-        return send_block(w, h, src, source, side_send.at[w, h, src // 2], beside)
-
-    def held(w, h):
-        return remote(own(w, h, 1 - y, 1 - odd), staged.at[held_rows(w, h), :], stage_send.at[w, h, 1], stage_recv.at[w, h], across)
+    def send_block(w, h, src, source, device, recv, send):
+        return remote(source, block(w, h, src), send.at[0], recv, device)
+
+    def line_sem(w, h, role):
+        return line_recv.at[w if h == 0 else 3, role]
+
+    def held_sem(w, h):
+        return held_recv.at[w if h == 0 else 3]
+
+    def block_in(w, h, sem):
+        if h == 0:
+            got(weights.at[pl.ds(0, sizes[0]), pl.ds(0, depth)], sem)
+        elif w == 0:
+            got(weights.at[pl.ds(0, 3 * sizes[1]), pl.ds(0, depth)], sem)
+
+    def to_near(w, h, src, source, line):
+        send_block(w, h, src, source, chip(x, y, near), line_sem(w, h, 1 + line), block_send).start()
+
+    def to_far(w, h, src, source, line):
+        send_block(w, h, src, source, chip(x, y, far), line_sem(w, h, 3 + line), block_send).start()
+
+    def to_other(w, h, src, source, line):
+        @pl.when(inner)
+        def _():
+            send_block(w, h, src, source, chip(x, y, other), line_sem(w, h, 5 + line), inner_send).start()
+
+    def pass_far(w, h, src, source, line):
+        @pl.when(inner)
+        def _():
+            send_block(w, h, src, source, chip(x, y, far), line_sem(w, h, 5 + line), inner_send).start()
+
+    def side(w, h, src, source, bundle):
+        send_block(w, h, src, source, beside, side_recv.at[h, bundle], block_send).start()
 
     def send_stage(h, some=range(3)):
         for w in some:
-            send_block(w, h, fs, own(w, h, 1 - y, odd), stage_send.at[w, h, 0], across).start()
-            held(w, h).start()
+            send_block(w, h, fs, own(w, h, 1 - y, odd), across, line_sem(w, h, 0), block_send).start()
+            remote(
+                own(w, h, 1 - y, 1 - odd), staged.at[held_rows(w, h), :], block_send.at[0], held_sem(w, h), across
+            ).start()
 
     def send_own(h, some=range(3)):
         for w in some:
-            send_block(w, h, fs, own(w, h, y, 1 - odd), near_send.at[w, h, 0], chip(x, y, near)).start()
-            send_block(w, h, fs, own(w, h, y, odd), far_send.at[w, h, 0], chip(x, y, far)).start()
-
-            @pl.when(inner)
-            def _():
-                send_block(w, h, fs, own(w, h, y, 1 - odd), other_send.at[w, h, 0], chip(x, y, other)).start()
-
-            side(w, h, fs, own(w, h, y, odd)).start()
+            to_near(w, h, fs, own(w, h, y, 1 - odd), 0)
+            to_far(w, h, fs, own(w, h, y, odd), 0)
+            side(w, h, fs, own(w, h, y, odd), 0)
+
+    def send_others(h):
+        for w in range(3):
+            to_other(w, h, fs, own(w, h, y, 1 - odd), 0)
+        for w in range(3):
+            to_other(w, h, z * 4 + (1 - y) * 2 + x, staged.at[held_rows(w, h), :], 1)
 
     def keep_own(h):
         for w in range(3):
@@ -202,33 +232,24 @@
 
     def stage_in(w, h):
         src = z * 4 + (1 - y) * 2 + x
-        held(w, h).wait_recv()
-        send_block(w, h, src, staged.at[held_rows(w, h), :], near_send.at[w, h, 1], chip(x, y, near)).start()
-
-        @pl.when(inner)
-        def _():
-            send_block(w, h, src, staged.at[held_rows(w, h), :], other_send.at[w, h, 1], chip(x, y, other)).start()
-
-        block_in(w, h, src)
-        send_block(w, h, src, block(w, h, src), far_send.at[w, h, 1], chip(x, y, far)).start()
-        side(w, h, src, block(w, h, src)).start()
-
-    def line_in(h, s, line):
+        held = staged.at[held_rows(w, h), :]
+        block_in(w, h, held_sem(w, h))
+        to_near(w, h, src, held, 1)
+        block_in(w, h, line_sem(w, h, 0))
+        to_far(w, h, src, block(w, h, src), 1)
+        side(w, h, src, block(w, h, src), 0)
+
+    def line_in(h, group, passed=None):
+        s, line, role, bundle = group
         for w in range(3):
             src = s * 4 + line * 2 + x
-            block_in(w, h, src)
-            if s is near:
-
-                @pl.when(inner)
-                def _():
-                    send_block(w, h, src, block(w, h, src), pass_send.at[w, h, int(line is not y)], chip(x, y, far)).start()
-
-            side(w, h, src, block(w, h, src)).start()
+            block_in(w, h, line_sem(w, h, role))
+            if passed is not None:
+                pass_far(w, h, src, block(w, h, src), passed)
+            side(w, h, src, block(w, h, src), bundle)
 
     def sides_in(h, groups):
-        for w in range(3):
-            for s, line in groups:
-                block_in(w, h, s * 4 + line * 2 + 1 - x)
+        got(weights.at[pl.ds(0, 3 * sizes[h]), pl.ds(0, len(groups) * depth)], side_recv.at[h, groups[0][3]])
 
     me = y * 2 + odd
     at_near, at_across, at_both = y * 2 + 1 - odd, (1 - y) * 2 + odd, (1 - y) * 2 + 1 - odd
@@ -236,18 +257,26 @@
     def token_rows(a, at):
         return grad_ref.at[at, :] if a == 2 else normed.at[a, at, :]
 
-    def tok_block(a, h, q):
-        return toks.at[a, pl.ds(pl.multiple_of(h * slab + q * half, half), half), :]
-
-    def tok_copy(a, n, q, source, device):
-        return remote(source, tok_block(a, core, q), tok_send.at[a, n], tok_recv.at[a, q], device)
-
-    def relay(a, q):
-        return remote(tok_block(a, core, q), tok_block(a, core, q), relay_send.at[a, q], relay_recv.at[a, q], sibling)
-
-    def send_tokens(a, n):
-        mine = token_rows(a, pl.ds(pl.multiple_of(core * half, half), half))
-        tok_copy(a, n, me, mine, (chip(x, y, near), across)[n]).start()
+    def tok_block(a, h, q, n=None):
+        rows_of = half if n is None else half // 2
+        first = h * slab + q * half + (0 if n is None else n * rows_of)
+        return toks.at[a, pl.ds(pl.multiple_of(first, rows_of), rows_of), :]
+
+    def tok_copy(a, q, source, device, role, n=None):
+        return remote(source, tok_block(a, core, q, n), tok_send.at[0], tok_recv.at[a, role], device)
+
+    def relay(a, q, n=None):
+        block_of = tok_block(a, core, q, n)
+        return remote(block_of, block_of, tok_send.at[0], relay_recv.at[a], sibling)
+
+    def tok_pieces(a):
+        return (None,) if a != 1 else (0, 1)
+
+    def send_tokens(a, role):
+        for n in tok_pieces(a) if role == 0 else (None,):
+            rows_of = half if n is None else half // 2
+            mine = token_rows(a, pl.ds(pl.multiple_of(core * half + (n or 0) * rows_of, rows_of), rows_of))
+            tok_copy(a, me, mine, (chip(x, y, near), across)[role], role + 3 * (n or 0), n).start()
 
     def normal(a):
         @pl.loop(0, tokens_ref.shape[0] // 16)
@@ -260,14 +289,15 @@
             toks[a, pl.ds(pl.multiple_of(h * slab + me * half, half), half), :] = token_rows(a, pl.ds(h * half, half))[...]
 
     def tok_in(a, q):
-        tok_copy(a, 0, q, tok_block(a, core, q), sibling).wait_recv()
-        if q is at_near:
-            tok_copy(a, 2, q, tok_block(a, core, q), across).start()
-        relay(a, q).start()
+        role = [q is at for at in (at_near, at_across, at_both)].index(True)
+        for n in tok_pieces(a) if role != 1 else (None,):
+            got(tok_block(a, core, q, n), tok_recv.at[a, role + 3 * (n or 0)])
+            if role == 0:
+                tok_copy(a, q, tok_block(a, core, q, n), across, 2 + 3 * (n or 0), n).start()
+            relay(a, q, n).start()
 
     def relayed(a):
-        for q in (at_near, at_across, at_both):
-            remote(tok_block(a, 1 - core, q), tok_block(a, 1 - core, q), relay_send.at[a, q], relay_recv.at[a, q], sibling).wait_recv()
+        got(toks.at[a, pl.ds(0, 3 * half), :], relay_recv.at[a])
 
     def project(h, kind, groups, first=False):
         a, w, count, into = ((0, 0, 2, back_acc), (2, 2, 1, down_acc), (1, 0, 2, fwd_acc))[kind]
@@ -276,7 +306,7 @@
         for t in range(2):
             at_tokens = pl.ds(t * slab, slab)
             value = None if first else into[h, at_tokens, :wide]
-            for s, line in groups:
+            for s, line, _, _ in groups:
                 at = pl.ds(pl.multiple_of((s * 4 + line * 2) * depth, 2 * depth), 2 * depth)
                 term = wide_dot(toks[a, at_tokens, at], weights[at_rows, at])
                 value = term if value is None else value + term
@@ -313,7 +343,7 @@
     def grad_across(h, n):
         pair = pl.ds((other, far, near, z)[n] * 2, 2)
         return remote(
-            grad_send.at[1 - x, pair, grad_rows(h)], grad_side.at[pair, grad_rows(h)], gside_send.at[h, n], gside_recv.at[h, n], beside
+            grad_send.at[1 - x, pair, grad_rows(h)], grad_side.at[pair, grad_rows(h)], gside_send.at[0], gside_recv.at[h, n], beside
         )
 
     def grad_make(h):
@@ -332,15 +362,15 @@
     def grad_to(h, n):
         s = (near, far, other)[n]
         source = grad_total.at[pl.ds(s * 2, 2), grad_rows(h)]
-        return remote(source, grad_recv.at[n, :, grad_rows(h)], glev_send.at[h, n], glev_recv.at[h, n], chip(x, y, s))
+        return remote(source, grad_recv.at[n, :, grad_rows(h)], gsend.at[0], glev_recv.at[h, n], chip(x, y, s))
 
     def grad_past(h):
         source = grad_total.at[pl.ds(other * 2, 2), grad_rows(h)]
-        return remote(source, grad_pass.at[:, grad_rows(h)], gpass_send.at[h], gpass_recv.at[h], chip(x, y, far))
+        return remote(source, grad_pass.at[:, grad_rows(h)], gsend.at[0], gpass_recv.at[h], chip(x, y, far))
 
     def grad_turned(h):
         return remote(
-            grad_turn.at[:, grad_rows(h)], turn_recv.at[:, grad_rows(h)], gturn_send.at[h], gturn_recv.at[h], across
+            grad_turn.at[:, grad_rows(h)], turn_recv.at[:, grad_rows(h)], gsend.at[0], gturn_recv.at[h], across
         )
 
     def grad_on(h, n):
@@ -417,7 +447,7 @@
     def cross(k, c):
         at = columns(c)
         return remote(
-            part.at[k, 1 - core, :, at], crossed.at[k, :, at], cross_sem.at[k, c, 0], cross_sem.at[k, c, 1], sibling
+            part.at[k, 1 - core, :, at], crossed.at[k, :, at], cross_send.at[0], cross_recv.at[k, c], sibling
         )
 
     strip = 512
@@ -442,7 +472,8 @@
             source, device = folded.at[k, :, at], on
         else:
             source, device = joined.at[k, (at_both, theirs)[n], :, at], to
-        return remote(source, gathered.at[k, n, :, at], join_send.at[k, c, n], join_recv.at[k, c, n], device)
+        recv = fold_recv.at[k, c] if n == 0 else join_recv.at[k]
+        return remote(source, gathered.at[k, n, :, at], join_send.at[0], recv, device)
 
     def join_start(k, c):
         cross(k, c).wait_recv()
@@ -465,12 +496,15 @@
         for w in range(3):
             stage_in(w, h)
 
-    first_far = (jnp.where(inner, other, far), jnp.where(inner, y, y_flip))
-    next_far = (other, jnp.where(inner, y_flip, y))
-    last_far = (jnp.where(inner, far, other), y_flip)
-    home = ((z, y), (z, y_flip))
-    soon = ((near, y), (far, y), first_far)
-    late = ((near, y_flip), next_far, last_far)
+    first_far = (jnp.where(inner, other, far), jnp.where(inner, y, y_flip), jnp.where(inner, 5, 4), 1)
+    next_far = (other, jnp.where(inner, y_flip, y), jnp.where(inner, 6, 5), 2)
+    last_far = (jnp.where(inner, far, other), y_flip, jnp.where(inner, 4, 6), 2)
+    near_own, near_across, far_own = (near, y, 1, 1), (near, y_flip, 2, 2), (far, y, 3, 1)
+    lead = (jnp.where(inner, near, far), jnp.where(inner, y, y_flip), jnp.where(inner, 1, 4), 1)
+    follow = (jnp.where(inner, other, near), y, jnp.where(inner, 5, 1), 1)
+    home = ((z, y, 0, 0), (z, y_flip, 0, 0))
+    soon = (near_own, far_own, first_far)
+    late = (near_across, next_far, last_far)
 
     def down_parts(k):
         for c in range(2):
@@ -501,41 +535,65 @@
     for a in range(3):
         keep_tokens(a)
     stages_in(0)
+    line_in(0, far_own)
+    line_in(0, lead, 0)
+    send_others(0)
+    send_stage(1)
+    tok_in(2, at_across)
+
+    @pl.when(inner)
+    def _():
+        tok_in(2, at_near)
+
+    line_in(0, follow)
+
+    @pl.when(jnp.logical_not(inner))
+    def _():
+        tok_in(2, at_near)
+
+    tok_in(0, at_across)
+    line_in(1, far_own)
+
+    @pl.when(inner)
+    def _():
+        tok_in(0, at_near)
+
+    stages_in(1)
     send_tokens(1, 0)
-    line_in(0, near, y)
-    line_in(0, far, y)
-    tok_in(2, at_across)
-    tok_in(2, at_near)
-    send_stage(1)
-    line_in(0, *first_far)
-    tok_in(0, at_across)
-    line_in(1, far, y)
-    tok_in(0, at_near)
+    send_others(1)
+    line_in(0, next_far)
+
+    @pl.when(jnp.logical_not(inner))
+    def _():
+        tok_in(0, at_near)
+
     send_tokens(1, 1)
-    line_in(0, *next_far)
-    line_in(1, near, y)
-    stages_in(1)
+    line_in(1, near_own, 0)
     tok_in(2, at_both)
-    line_in(0, near, y_flip)
+    line_in(0, near_across, 1)
     relayed(2)
-    line_in(1, *first_far)
+    line_in(1, first_far)
     sides_in(0, home)
     project(0, 1, home, True)
     tok_in(0, at_both)
-    line_in(1, *next_far)
+    line_in(1, next_far)
     relayed(0)
     project(0, 0, home, True)
     tok_in(1, at_across)
     sides_in(0, soon)
     project(0, 1, soon)
-    line_in(0, *last_far)
+    line_in(0, last_far)
     project(0, 0, soon)
-    tok_in(1, at_near)
+
+    @pl.when(inner)
+    def _():
+        tok_in(1, at_near)
+
     sides_in(1, home)
     project(1, 0, home, True)
     project(1, 1, home, True)
-    line_in(1, near, y_flip)
-    line_in(1, *last_far)
+    line_in(1, near_across, 1)
+    line_in(1, last_far)
     sides_in(1, soon)
     project(1, 0, soon)
     project(1, 1, soon)
@@ -545,16 +603,21 @@
     back_parts(0)
     grad_make(0)
     grad_out(0)
-    tok_in(1, at_both)
+
+    @pl.when(jnp.logical_not(inner))
+    def _():
+        tok_in(1, at_near)
+
     sides_in(1, late)
     project(1, 0, late)
     project(1, 1, late)
     back_parts(1)
     down_parts(1)
+    for c in range(2):
+        join_start(1, c)
     grad_make(1)
     grad_out(1)
-    for c in range(2):
-        join_start(1, c)
+    tok_in(1, at_both)
     relayed(1)
     project(0, 2, home + soon + late, True)
     fwd_parts(0)
@@ -566,15 +629,15 @@
     for c in range(2):
         join_start(0, c)
     grad_on(0, 2)
+    for c in range(2):
+        join_fold(1, c)
     grad_on(0, 3)
     grad_mid(0)
-    for c in range(2):
-        join_fold(1, c)
     for n in range(4):
         grad_on(1, n)
-    grad_mid(1)
     for c in range(2):
         join_fold(0, c)
+    grad_mid(1)
     grad_cross(0)
     grad_cross(1)
 
@@ -582,12 +645,10 @@
 
     def last(k):
         out = (fwd_out, back_out)[k].at[mine, :]
-        return remote(out, out, last_sem.at[k, 0], last_sem.at[k, 1], sibling)
+        return remote(out, out, last_send.at[0], last_recv.at[0], sibling)
 
     def joined_in(k):
-        for c in range(2):
-            for n in (1, 2):
-                join_copy(k, c, n).wait_recv()
+        got(gathered.at[k, pl.ds(1, 2)], join_recv.at[k])
 
     def total_of(k, at):
         value = joined[k, me, at, :].astype(jnp.float32) + gathered[k, 1, at, :].astype(jnp.float32)
@@ -628,47 +689,19 @@
         grad_in(h)
     grad_tiles((1 - y) * early, tiles - early)
 
-    for h in range(2):
-        for w in range(3):
-            for n in range(2):
-                gone = block(w, h, fs)
-                for sem in (stage_send, near_send, far_send):
-                    send_block(w, h, fs, gone, sem.at[w, h, n], sibling).wait_send()
-
-                @pl.when(inner)
-                def _():
-                    for sem in (other_send, pass_send):
-                        send_block(w, h, fs, gone, sem.at[w, h, n], sibling).wait_send()
-
-            @pl.loop(0, 8)
-            def _(j):
-                send_block(w, h, fs, gone, side_send.at[w, h, j], sibling).wait_send()
-
-        for s in range(4):
-            grad_across(h, s).wait_send()
-        grad_to(h, 0).wait_send()
-        grad_to(h, 1).wait_send()
-        grad_turned(h).wait_send()
-
-        @pl.when(inner)
-        def _():
-            grad_to(h, 2).wait_send()
-
-        @pl.when(jnp.logical_not(inner))
-        def _():
-            grad_past(h).wait_send()
-
-    for a in range(3):
-        for n in range(3):
-            tok_copy(a, n, me, tok_block(a, core, me), sibling).wait_send()
-        for q in (at_near, at_across, at_both):
-            relay(a, q).wait_send()
-    for k in range(2):
-        for c in range(2):
-            cross(k, c).wait_send()
-            for n in range(3):
-                join_copy(k, c, n).wait_send()
-        last(k).wait()
+    gone(weights.at[pl.ds(0, 3 * rows), pl.ds(0, 14 * depth)], block_send.at[0])
+
+    @pl.when(inner)
+    def _():
+        gone(weights.at[pl.ds(0, 3 * rows), pl.ds(0, 4 * depth)], inner_send.at[0])
+
+    gone(toks.at[:, pl.ds(0, 6 * half), :], tok_send.at[0])
+    gone(grad_side, gside_send.at[0])
+    gone(grad_total, gsend.at[0])
+    gone(part.at[0], cross_send.at[0])
+    gone(joined.at[:, pl.ds(0, 3)], join_send.at[0])
+    gone(fwd_out, last_send.at[0])
+    got(fwd_out, last_recv.at[0])
 
 
 def fused_shards(
@@ -723,30 +756,27 @@
             pltpu.VMEM((2, rows, depth), narrow),
             pltpu.VMEM((2, rows, depth), narrow),
             pltpu.VMEM((cols, depth), full),
-            dma((3, 2, 2)),
-            dma((3, 2)),
-            dma((3, 2, 16)),
-            dma((3, 2, 2)),
-            dma((3, 2, 2)),
-            dma((3, 2, 2)),
-            dma((3, 2, 2)),
-            dma((3, 2, 8)),
-            dma((3, 3)),
-            dma((3, 4)),
-            dma((3, 4)),
-            dma((3, 4)),
+            dma((1,)),
+            dma((1,)),
+            dma((4, 7)),
+            dma((4,)),
+            dma((2, 3)),
+            dma((1,)),
+            dma((3, 6)),
+            dma((3,)),
+            dma((1,)),
             dma((2, 4)),
-            dma((2, 4)),
-            dma((2, 3)),
+            dma((1,)),
             dma((2, 3)),
             dma((2,)),
             dma((2,)),
+            dma((1,)),
+            dma((2, 2)),
+            dma((1,)),
+            dma((2, 2)),
             dma((2,)),
-            dma((2,)),
-            dma((2, 2, 2)),
-            dma((2, 2, 3)),
-            dma((2, 2, 3)),
-            dma((2, 2)),
+            dma((1,)),
+            dma((1,)),
             dma((3,)),
             dma((3,)),
             dma((1,)),

time: 104 us -> 97.5 us (0.938)
  Pallas kernels: 101 us -> 94.2 us
    pallas_call x1, Pallas kernels: 101 us -> 94.2 us  [fused_shards(): pl.pallas_call(functools.partial(layer_kernel, split), out_shape=(pltpu.V...]
where the time goes in v4:
time: 97.5 us; the launch traced here: 97.3 us
  Pallas kernels  94.2 us (97%)
  local copies, waits for them, and re-layouts  2.45 us (3%)
    pallas_call x1, Pallas kernels, fused_shards(): pl.pallas_call(functools.partial(layer_kernel, split), out_shape=(pltpu.V...  94.2 us
    unnamed x3, local copies, waits for them, and re-layouts  2.45 us

profile of v4, /device:TPU:0, one launch (start us, length us, event | category | flops | bytes accessed | tf_op | source)
XLA Modules:
  0.0 97.3 jit_solution(12444265900835009822)
XLA Ops:
  0.6 94.2 %shard_map.103 = (bf16[128,2048]{1,0:T(8,128)(2,1)S(1)}, bf16[128,2048]{1,0:T(8,128)(2,1)S(1)}, f32[128,1408]{1,0:T(8,128)S(1)}) custom-call(bf16[128,2048]{1,0:T(8,128)(2,1)} %fwd_in.1, bf16[128,2048]{1,0:T(8,128)(2,1)} %tokens_in.1, bf16[128,2048]{1,0:T(8,128)(2,1)} %grad_in_ref.1, f32[1,2048]{1,0:T(1,128)} %bitcast.1, bf16[128,1408]{1,0:T(8,128)(2,1)} %gate_in.1, ...), custom_call_target="tpu_custom_call" | custom-call | tf_op jit(solution)/shard_map/pallas_call | solution.py:722
  94.9 0.8 copy.14
  95.7 0.8 copy.15
  96.5 0.9 copy.16

commit v5 on v4

--- a/solution.py
+++ b/solution.py
@@ -476,14 +476,19 @@
         return remote(source, gathered.at[k, n, :, at], join_send.at[0], recv, device)
 
     def join_start(k, c):
-        cross(k, c).wait_recv()
-        at = columns(c)
-        for n, q in enumerate((at_both, *routes[routed[k][c]][1:3], me)):
-            rows_at = pl.ds(pl.multiple_of(q * half, half), half)
-            total = part[k, core, rows_at, at].astype(jnp.float32) + crossed[k, rows_at, at].astype(jnp.float32)
-            joined[k, q, :, at] = total.astype(jnp.bfloat16)
-            if n < 2:
-                join_copy(k, c, n).start()
+        if c == 0:
+            return
+        for c in range(2):
+            cross(k, c).wait_recv()
+        for n in range(4):
+            for c in range(2):
+                at = columns(c)
+                q = (at_both, *routes[routed[k][c]][1:3], me)[n]
+                rows_at = pl.ds(pl.multiple_of(q * half, half), half)
+                total = part[k, core, rows_at, at].astype(jnp.float32) + crossed[k, rows_at, at].astype(jnp.float32)
+                joined[k, q, :, at] = total.astype(jnp.bfloat16)
+                if n < 2:
+                    join_copy(k, c, n).start()
 
     def join_fold(k, c):
         at = columns(c)
@@ -615,20 +620,20 @@
     down_parts(1)
     for c in range(2):
         join_start(1, c)
-    grad_make(1)
-    grad_out(1)
     tok_in(1, at_both)
+    grad_on(0, 0)
     relayed(1)
     project(0, 2, home + soon + late, True)
     fwd_parts(0)
-    grad_on(0, 0)
+    grad_on(0, 1)
     project(1, 2, home + soon + late, True)
     fwd_parts(1)
     down_parts(0)
-    grad_on(0, 1)
+    grad_on(0, 2)
     for c in range(2):
         join_start(0, c)
-    grad_on(0, 2)
+    grad_make(1)
+    grad_out(1)
     for c in range(2):
         join_fold(1, c)
     grad_on(0, 3)

time: 97.5 us -> 96.3 us (0.988)
  Pallas kernels: 94.2 us -> 93 us
    pallas_call x1, Pallas kernels: 94.2 us -> 93 us  [fused_shards(): pl.pallas_call(functools.partial(layer_kernel, split), out_shape=(pltpu.V...]
where the time goes in v5:
time: 96.3 us; the launch traced here: 96.1 us
  Pallas kernels  93 us (97%)
  local copies, waits for them, and re-layouts  2.45 us (3%)
    pallas_call x1, Pallas kernels, fused_shards(): pl.pallas_call(functools.partial(layer_kernel, split), out_shape=(pltpu.V...  93 us
    unnamed x3, local copies, waits for them, and re-layouts  2.45 us

profile of v5, /device:TPU:0, one launch (start us, length us, event | category | flops | bytes accessed | tf_op | source)
XLA Modules:
  0.0 96.1 jit_solution(13816124943292246093)
XLA Ops:
  0.6 93.0 %shard_map.103 = (bf16[128,2048]{1,0:T(8,128)(2,1)S(1)}, bf16[128,2048]{1,0:T(8,128)(2,1)S(1)}, f32[128,1408]{1,0:T(8,128)S(1)}) custom-call(bf16[128,2048]{1,0:T(8,128)(2,1)} %fwd_in.1, bf16[128,2048]{1,0:T(8,128)(2,1)} %tokens_in.1, bf16[128,2048]{1,0:T(8,128)(2,1)} %grad_in_ref.1, f32[1,2048]{1,0:T(1,128)} %bitcast.1, bf16[128,1408]{1,0:T(8,128)(2,1)} %gate_in.1, ...), custom_call_target="tpu_custom_call" | custom-call | tf_op jit(solution)/shard_map/pallas_call | solution.py:727
  93.6 0.8 copy.14
  94.4 0.8 copy.15
  95.2 0.9 copy.16

commit v6 on v5

--- a/solution.py
+++ b/solution.py
@@ -663,8 +663,7 @@
     early = rows * 2 // 128
 
     def grad_tiles(first, count):
-        @pl.loop(0, count)
-        def _(n):
+        for n in range(count):
             at = pl.ds(pl.multiple_of((first + n) * 128, 128), 128)
             sum_out[:, at] = sum_ref[:, at] + grad_cols[at, :].T
 

time: 96.3 us -> 96.3 us (level)
  no operation moved by 1% of the time
where the time goes in v6:
time: 96.3 us; the launch traced here: 95.7 us
  Pallas kernels  92.6 us (96%)
  local copies, waits for them, and re-layouts  2.45 us (3%)
    pallas_call x1, Pallas kernels, fused_shards(): pl.pallas_call(functools.partial(layer_kernel, split), out_shape=(pltpu.V...  92.6 us
    unnamed x3, local copies, waits for them, and re-layouts  2.45 us

profile of v6, /device:TPU:0, one launch (start us, length us, event | category | flops | bytes accessed | tf_op | source)
XLA Modules:
  0.0 95.7 jit_solution(6628909435904946820)
XLA Ops:
  0.6 92.6 %shard_map.103 = (bf16[128,2048]{1,0:T(8,128)(2,1)S(1)}, bf16[128,2048]{1,0:T(8,128)(2,1)S(1)}, f32[128,1408]{1,0:T(8,128)S(1)}) custom-call(bf16[128,2048]{1,0:T(8,128)(2,1)} %fwd_in.1, bf16[128,2048]{1,0:T(8,128)(2,1)} %tokens_in.1, bf16[128,2048]{1,0:T(8,128)(2,1)} %grad_in_ref.1, f32[1,2048]{1,0:T(1,128)} %bitcast.1, bf16[128,1408]{1,0:T(8,128)(2,1)} %gate_in.1, ...), custom_call_target="tpu_custom_call" | custom-call | tf_op jit(solution)/shard_map/pallas_call | solution.py:726
  93.3 0.8 copy.14
  94.1 0.8 copy.15
  94.9 0.9 copy.16
